TPU v7x, 32 devices: a whole 2x2x4 slice. The times are simulated.
32 devices in a mesh: ep: 16 (over z, y, x), tp: 2 (over core).
Axes of the slice: x: 2, y: 2, z: 4, core: 2. Of those that a mesh axis runs over, the one named last changes fastest.
Arguments:
- tokens: bfloat16 [256, 2048], P(('ep', 'tp')), may hold values from -6 to 6
- mix_gain: float32 [2048], replicated, may hold values from 0.1 to 1.9
- w_query: bfloat16 [2048, 16, 128], P(None, 'tp', 'ep'), may hold values from -0.125 to 0.125
- w_key: bfloat16 [2048, 16, 128], P(None, 'tp', 'ep'), may hold values from -0.125 to 0.125
- w_value: bfloat16 [2048, 16, 128], P(None, 'tp', 'ep'), may hold values from -0.125 to 0.125
- w_zgate: bfloat16 [2048, 16, 128], P(None, 'tp', 'ep'), may hold values from -0.125 to 0.125
- w_beta: bfloat16 [2048, 16], P(None, 'tp'), may hold values from -0.125 to 0.125
- w_decay: bfloat16 [2048, 16], P(None, 'tp'), may hold values from -0.125 to 0.125
- decay_rate: float32 [16], P('tp'), may hold values from 0.5 to 8
- decay_bias: float32 [16], P('tp'), may hold values from -3 to 0
- head_gain: float32 [128], replicated, may hold values from 0.1 to 1.9
- state: float32 [256, 16, 128, 128], P('ep', 'tp'), may hold values from -1.5 to 1.5
- w_out: bfloat16 [2048, 2048], P('tp', 'ep'), may hold values from -0.125 to 0.125
- moe_gain: float32 [2048], replicated, may hold values from 0.1 to 1.9
- dense_mix: bfloat16 [2048], replicated, may hold values from -0.125 to 0.125
- dense_gate: bfloat16 [2048, 4096], P(None, ('ep', 'tp')), may hold values from -0.125 to 0.125
- dense_up: bfloat16 [2048, 4096], P(None, ('ep', 'tp')), may hold values from -0.125 to 0.125
- dense_down: bfloat16 [4096, 2048], P(('ep', 'tp')), may hold values from -0.09375 to 0.09375
- expert_gate: bfloat16 [16, 2048, 1024], P('ep', None, 'tp'), may hold values from -0.125 to 0.125
- expert_up: bfloat16 [16, 2048, 1024], P('ep', None, 'tp'), may hold values from -0.125 to 0.125
- expert_down: bfloat16 [16, 1024, 2048], P('ep', 'tp'), may hold values from -0.1875 to 0.1875
- expert_ids: int32 [256, 4], replicated, may hold values from 0 to 15, as said below
- route_weight: float32 [256, 4], replicated, may hold values from 0.1 to 1
Outputs:
- layer_out: bfloat16 [256, 2048], P(('ep', 'tp'))
- new_state: float32 [256, 16, 128, 128], P('ep', 'tp')
Inputs may be any that keep to these rules, and one draw needn't show every extreme that they name: `expert_ids`: the 4 experts of a row are distinct and lie in one group of 8 consecutive ids. In each aligned block of 16 rows (the rows of one index of ep) no expert is named by more than 8 rows, and at most 16 rows pick one group.
All inputs are finite; a program needn't handle non-finite values.
Results may differ from a plain program's by a relative error of at most 0.012.
Values may be sent and summed in bfloat16 or wider, within the bound.
A program may use at most 128 MiB of HBM per device.

v0:
```python
import functools

import jax
import jax.numpy as jnp
from jax import lax
from jax.experimental import pallas as pl
from jax.experimental.pallas import tpu as pltpu
from jax.sharding import PartitionSpec as P

EPS = 1e-06
VMEM = pltpu.VMEM
MESH = pl.DeviceIdType.MESH


def rms_scale(values, gain):
    return values * lax.rsqrt(jnp.mean(values * values, axis=-1, keepdims=True) + EPS) * gain


def grid_of(count):
    for depth in (4, 2, 1):
        side = int(round((count / depth) ** 0.5))
        if depth * side * side == count:
            return depth, side
    return count, 1


def place(count):
    depth, side = grid_of(count)
    ep = lax.axis_index("ep")
    t = lax.axis_index("tp")
    z = ep // (side * side)
    y = (ep // side) % side
    x = ep % side
    a = x * (1 - t) + y * t
    b = y * (1 - t) + x * t
    return depth, side, t, z, b, a


def ep_of(side, t, z, b, a):
    y = b * (1 - t) + a * t
    x = a * (1 - t) + b * t
    return (z * side + y) * side + x


def near(count):
    depth, side, t, z, b, a = place(count)
    steps = [(lax.rem(z + i, depth), b, a) for i in range(1, depth)]
    steps += [(z, lax.rem(b + i, side), a) for i in range(1, side)]
    steps += [(z, b, lax.rem(a + i, side)) for i in range(1, side)]
    return [(ep_of(side, t, *c), t) for c in steps]


def gather_phase(count, both, block_ref, out_ref, send_sem, recv_sem):
    depth, side, t, z, b, a = place(count)
    zs = [((lax.rem(z + i, depth)), b, a) for i in range(1, depth)]
    bs = [(z, lax.rem(b + i, side), a) for i in range(1, side)]
    as_ = [(z, b, lax.rem(a + i, side)) for i in range(1, side)]
    device_of = lambda c: (ep_of(side, t, *c), t)
    partner = (lax.axis_index("ep"), 1 - t)
    width = 2 if both else 1
    slot_of = lambda dz, db, da: (
        ep_of(side, t, lax.rem(z + dz, depth), lax.rem(b + db, side), lax.rem(a + da, side)) * width
        + (t if both else 0)
    )
    mine = slot_of(0, 0, 0)
    out_ref[mine] = block_ref[...]
    counter = [0]
    started = []
    arrivals = {}

    def send(src, offset, key, device):
        number = counter[0]
        counter[0] += 1
        copy = pltpu.make_async_remote_copy(
            src_ref=src,
            dst_ref=out_ref.at[slot_of(*offset)],
            send_sem=send_sem.at[number],
            recv_sem=recv_sem.at[number],
            device_id=device,
            device_id_type=MESH,
        )
        copy.start()
        started.append(copy)
        arrivals[key] = copy

    def relay(offset, legs):
        dz, db, da = offset
        src = block_ref if offset == (0, 0, 0) else out_ref.at[slot_of(*offset)]
        if "a" in legs:
            for i in range(1, side):
                send(src, offset, ("a", (dz, db, (da - i) % side)), device_of(as_[i - 1]))
        if "b" in legs:
            for i in range(1, side):
                send(src, offset, ("b", (dz, (db - i) % side, da)), device_of(bs[i - 1]))
        if "z" in legs:
            for i in range(1, depth):
                send(src, offset, ("z", ((dz - i) % depth, db, da)), device_of(zs[i - 1]))
        if both:
            send(src, offset, ("t", offset), partner)

    relay((0, 0, 0), "zba")
    for dz in range(1, depth):
        arrivals["z", (dz, 0, 0)].wait_recv()
        relay((dz, 0, 0), "ba")
    for dz in range(depth):
        for db in range(1, side):
            arrivals["b", (dz, db, 0)].wait_recv()
            relay((dz, db, 0), "a")
    for dz in range(depth):
        for db in range(side):
            for da in range(1, side):
                arrivals["a", (dz, db, da)].wait_recv()
                relay((dz, db, da), "")
    if both:
        for key, copy in arrivals.items():
            if key[0] == "t":
                copy.wait_recv()
    for copy in started:
        copy.wait_send()


def copies_of(count, both):
    return count - 1 + (count if both else 0)


def device_at(count, both, i):
    t = lax.axis_index("tp")
    me = lax.axis_index("ep") * 2 + t if both else lax.axis_index("ep")
    other = lax.rem(me + i, count * 2 if both else count)
    return other, ((other // 2, other % 2) if both else (other, t))


def greet_all(count, both):
    barrier = pltpu.get_barrier_semaphore()

    def hello(i, carry):
        pl.semaphore_signal(
            barrier, inc=1, device_id=device_at(count, both, i)[1], device_id_type=MESH
        )
        return carry

    lax.fori_loop(1, count * 2 if both else count, hello, 0)


def exchange_phase(count, both, blocks_ref, out_ref, send_sem, recv_sem):
    total = count * 2 if both else count
    t = lax.axis_index("tp")
    me = lax.axis_index("ep") * 2 + t if both else lax.axis_index("ep")

    def copy(i):
        other, target = device_at(count, both, i)
        return pltpu.make_async_remote_copy(
            src_ref=blocks_ref.at[other],
            dst_ref=out_ref.at[me],
            send_sem=send_sem.at[i],
            recv_sem=recv_sem.at[i],
            device_id=target,
            device_id_type=MESH,
        )

    def start(i, carry):
        copy(i).start()
        return carry

    def finish(i, carry):
        copy(i).wait()
        return carry

    lax.fori_loop(1, total, start, 0)
    out_ref[me] = blocks_ref[me]
    lax.fori_loop(1, total, finish, 0)


def contract(left, right):
    return lax.dot_general(left, right, (((1,), (1,)), ((), ())), preferred_element_type=jnp.float32)


def flat_rows(ref):
    blocks, rows, width = ref.shape
    return ref[...].astype(jnp.float32).reshape(blocks * rows, width)


def project_kernel(
    count,
    tokens_ref,
    gain_ref,
    wq_ref,
    wk_ref,
    wv_ref,
    wz_ref,
    beta_ref,
    decay_ref,
    out_ref,
    rates_ref,
    own,
    rows,
    blocks,
    send_sem,
    recv_sem,
    send_sem2,
    recv_sem2,
):
    partner = (lax.axis_index("ep"), 1 - lax.axis_index("tp"))
    barrier = pltpu.get_barrier_semaphore()
    pl.semaphore_signal(barrier, inc=1, device_id=partner, device_id_type=MESH)
    greet_all(count, False)
    own[...] = rms_scale(tokens_ref[...].astype(jnp.float32), gain_ref[...]).astype(own.dtype)
    pl.semaphore_wait(barrier, count)
    gather_phase(count, True, own, rows, send_sem, recv_sem)
    flat = flat_rows(rows).astype(jnp.bfloat16)
    heads = beta_ref.shape[0]
    columns = wq_ref.shape[0]
    wide = 4 * columns
    source = lax.broadcasted_iota(jnp.int32, (columns, wide), 0)
    target = lax.broadcasted_iota(jnp.int32, (columns, wide), 1)
    moved = jnp.zeros((flat.shape[0], wide), jnp.float32)
    for p, w_ref in enumerate((wq_ref, wk_ref, wv_ref, wz_ref)):
        piece = contract(flat, w_ref[...]).astype(jnp.bfloat16)
        spot = source % (columns // heads) * (4 * heads) + p * heads + source // (columns // heads)
        order = jnp.where(target == spot, 1.0, 0.0).astype(jnp.bfloat16)
        moved = moved + jnp.dot(piece, order, preferred_element_type=jnp.float32)
    blocks[...] = moved.reshape(blocks.shape).astype(blocks.dtype)
    ep = lax.axis_index("ep")
    seq = jnp.concatenate(
        [rows[2 * ep].astype(jnp.float32), rows[2 * ep + 1].astype(jnp.float32)], axis=0
    ).astype(jnp.bfloat16)
    exchange_phase(count, False, blocks, out_ref, send_sem2, recv_sem2)
    rates_ref[:, :heads] = contract(seq, beta_ref[...])
    rates_ref[:, heads:] = contract(seq, decay_ref[...])


def sems(n):
    return [pltpu.SemaphoreType.DMA((n,)), pltpu.SemaphoreType.DMA((n,))]


def comm_call(kernel, number, out_shape, operands, scratch):
    spec = pl.BlockSpec(memory_space=VMEM)
    return pl.pallas_call(
        kernel,
        out_shape=out_shape,
        in_specs=[spec] * len(operands),
        out_specs=jax.tree.map(lambda _: spec, out_shape),
        scratch_shapes=scratch,
        compiler_params=pltpu.CompilerParams(
            collective_id=number, has_side_effects=True, vmem_limit_bytes=60 * 1024 * 1024
        ),
        name=f"stage_{number}",
    )(*operands)


def mix_kernel(
    count,
    gated_ref,
    w_ref,
    tokens_ref,
    gain_ref,
    resid_ref,
    all_ref,
    rows,
    parts,
    landed,
    own,
    send_sem,
    recv_sem,
    send_sem2,
    recv_sem2,
    send_sem3,
    recv_sem3,
):
    greet_all(count, True)
    pl.semaphore_wait(pltpu.get_barrier_semaphore(), 2 * count - 1)
    gather_phase(count, False, gated_ref, rows, send_sem, recv_sem)
    flat = flat_rows(rows).astype(jnp.bfloat16)
    product = jnp.dot(flat, w_ref[...], preferred_element_type=jnp.float32)
    parts[...] = product.reshape(parts.shape).astype(parts.dtype)
    exchange_phase(count, True, parts, landed, send_sem2, recv_sem2)
    mixed = [
        landed[2 * i].astype(jnp.float32) + landed[2 * i + 1].astype(jnp.float32)
        for i in range(count)
    ]
    resid = tokens_ref[...].astype(jnp.float32) + jnp.concatenate(mixed, axis=1)
    resid_ref[...] = resid
    own[...] = rms_scale(resid, gain_ref[...]).astype(own.dtype)
    gather_phase(count, True, own, all_ref, send_sem3, recv_sem3)


def scatter_phase(
    count, part_ref, core_buf, sum1, a_buf, sum2, b_buf, sum3, z_buf, send_sem, recv_sem
):
    depth, side, t, z, b, a = place(count)
    device_of = lambda dz, db, da: (
        ep_of(side, t, lax.rem(z + dz, depth), lax.rem(b + db, side), lax.rem(a + da, side)),
        t,
    )
    partner = (lax.axis_index("ep"), 1 - t)
    counter = [0]
    started = []

    def send(src, dst, device, number=None):
        if number is None:
            number = count + counter[0]
            counter[0] += 1
        copy = pltpu.make_async_remote_copy(
            src_ref=src,
            dst_ref=dst,
            send_sem=send_sem.at[number],
            recv_sem=recv_sem.at[number],
            device_id=device,
            device_id_type=MESH,
        )
        copy.start()
        started.append(copy)
        return copy

    add = lambda first, *rest: functools.reduce(
        lambda u, v: u + v, [w.astype(jnp.float32) for w in (first,) + rest]
    )
    order = [
        (dz, db, da)
        for da in list(range(1, side)) + [0]
        for db in list(range(1, side)) + [0]
        for dz in list(range(1, depth)) + [0]
    ]
    absolute = lambda dz, db, da: ep_of(
        side, t, lax.rem(z + dz, depth), lax.rem(b + db, side), lax.rem(a + da, side)
    )
    for dz, db, da in order:
        spot = absolute(dz, da, db)
        send(part_ref.at[spot * 2 + 1 - t], core_buf.at[spot], partner, spot)

    def core_arrival(spot):
        return pltpu.make_async_remote_copy(
            src_ref=part_ref.at[spot * 2 + 1 - t],
            dst_ref=core_buf.at[spot],
            send_sem=send_sem.at[spot],
            recv_sem=recv_sem.at[spot],
            device_id=partner,
            device_id_type=MESH,
        )

    a_copies = {}
    for c in order:
        dz, db, da = c
        core_arrival(absolute(*c)).wait_recv()
        total = add(part_ref[absolute(*c) * 2 + t], core_buf[absolute(*c)])
        slot = (da * side + db) * depth + dz
        sum1[slot] = total.astype(sum1.dtype)
        if da:
            a_copies[c] = send(
                sum1.at[slot], a_buf.at[(da * side + db) * depth + dz], device_of(0, 0, da)
            )
    b_copies = {}
    for db in list(range(1, side)) + [0]:
        for dz in list(range(1, depth)) + [0]:
            terms = [sum1[db * depth + dz]]
            for da in range(1, side):
                a_copies[dz, db, da].wait_recv()
                terms.append(a_buf[(da * side + db) * depth + dz])
            sum2[db * depth + dz] = add(*terms).astype(sum2.dtype)
            if db:
                b_copies[dz, db] = send(
                    sum2.at[db * depth + dz], b_buf.at[db * depth + dz], device_of(0, db, 0)
                )
    z_copies = []
    for dz in list(range(1, depth)) + [0]:
        terms = [sum2[dz]]
        for db in range(1, side):
            b_copies[dz, db].wait_recv()
            terms.append(b_buf[db * depth + dz])
        total = add(*terms)
        if dz:
            sum3[dz] = total.astype(sum3.dtype)
            z_copies.append(send(sum3.at[dz], z_buf.at[dz], device_of(dz, 0, 0)))
    for dz in range(1, depth):
        z_copies[dz - 1].wait_recv()
        total = total + z_buf[dz].astype(jnp.float32)
    for copy in started:
        copy.wait_send()
    return total


def moe_kernel(
    count,
    rows_ref,
    resid_ref,
    mix_ref,
    dg_ref,
    du_ref,
    dd_ref,
    eg_ref,
    eu_ref,
    ed_ref,
    ids_ref,
    route_ref,
    out_ref,
    part,
    *rest,
):
    ep = lax.axis_index("ep")
    partner = (ep, 1 - lax.axis_index("tp"))
    barrier = pltpu.get_barrier_semaphore()
    peers = [partner] + near(count)
    for device in peers:
        pl.semaphore_signal(barrier, inc=1, device_id=device, device_id_type=MESH)
    wide = flat_rows(rows_ref)
    total, width = wide.shape
    mix = 1.0 / (1.0 + jnp.exp(-jnp.sum(wide * mix_ref[...], axis=1, keepdims=True)))
    flat = wide.astype(jnp.bfloat16)
    weight = jnp.sum(jnp.where(ids_ref[...] == ep, route_ref[...], 0.0), axis=0, keepdims=True)
    line = lax.broadcasted_iota(jnp.int32, (total, total), 0)
    lane = lax.broadcasted_iota(jnp.int32, (total, total), 1)
    weight = jnp.sum(jnp.where(line == lane, weight, 0.0), axis=1, keepdims=True)

    def hidden(gate, up):
        gate = jnp.dot(flat, gate, preferred_element_type=jnp.float32)
        up = jnp.dot(flat, up, preferred_element_type=jnp.float32)
        return (gate / (1.0 + jnp.exp(-gate)) * up).astype(jnp.bfloat16)

    dense = hidden(dg_ref[...], du_ref[...])
    expert = hidden(eg_ref[...], eu_ref[...])
    step = min(512, width)
    for start in range(0, width, step):
        span = slice(start, start + step)
        term = mix * jnp.dot(dense, dd_ref[:, span], preferred_element_type=jnp.float32)
        term = term + weight * jnp.dot(expert, ed_ref[:, span], preferred_element_type=jnp.float32)
        part[:, :, span] = term.reshape(part.shape[0], part.shape[1], step).astype(part.dtype)
    pl.semaphore_wait(barrier, len(peers))
    total = scatter_phase(count, part, *rest)
    out_ref[...] = (resid_ref[...] + total).astype(out_ref.dtype)


def delta_kernel(
    heads, rate_ref, bias_ref, rates_ref, x_ref, gain_ref, state_ref, gated_ref, new_ref, cols_buf, acc
):
    seq = pl.program_id(0)
    count, wide = x_ref.shape[1:]
    part = wide // (4 * heads)
    size = count * part
    silu = lambda v: v / (1.0 + jnp.exp(-v))
    x = x_ref[0]
    for i in range(part):
        cols_buf[pl.ds(i, count, stride=part), :] = x[:, i * 4 * heads : (i + 1) * 4 * heads]
    cols = cols_buf[...]
    rows = silu(jnp.transpose(cols)[2 * heads :])
    cols = silu(cols)
    cols = cols * lax.rsqrt(jnp.sum(cols * cols, axis=0, keepdims=True) + EPS)
    value, gate = rows[:heads], rows[heads:]
    tall = lambda pick: jnp.concatenate(
        [jnp.full((1, size), pick(h), jnp.float32) for h in range(heads)], axis=0
    )
    beta = 1.0 / (1.0 + jnp.exp(-tall(lambda h: rates_ref[seq, h])))
    pre = tall(lambda h: rates_ref[seq, heads + h] + bias_ref[h])
    soft = jnp.maximum(pre, 0.0) + jnp.log1p(jnp.exp(-jnp.abs(pre)))
    retain = jnp.exp(-tall(lambda h: rate_ref[h]) * soft)
    readouts = []
    for h in range(heads):
        query = cols[:, h : h + 1] * size ** (-0.5)
        key = cols[:, heads + h : heads + h + 1]
        keep = retain[h : h + 1]
        old = state_ref[0, h]
        recalled = jnp.sum(old * key, axis=0, keepdims=True)
        correction = value[h : h + 1] - keep * recalled
        new = keep * old + key * (beta[h : h + 1] * correction)
        new_ref[0, h] = new
        readouts.append(jnp.sum(new * query, axis=0, keepdims=True))
    readout = jnp.concatenate(readouts, axis=0)
    gated = rms_scale(readout, gain_ref[...]) * gate
    acc[pl.ds(pl.multiple_of(seq * heads, heads), heads), :] = gated

    @pl.when(seq == pl.num_programs(0) - 1)
    def _():
        for h in range(heads):
            piece = acc[pl.ds(h, gated_ref.shape[0], stride=heads), :]
            gated_ref[:, h * size : (h + 1) * size] = piece.astype(gated_ref.dtype)


def delta(rate, bias, rates, x, gain, state):
    seqs, heads, size, _ = state.shape
    own = lambda *shape: pl.BlockSpec((1,) + shape, lambda s: (s,) + (0,) * len(shape))
    scalars = pl.BlockSpec(memory_space=pltpu.SMEM)
    return pl.pallas_call(
        functools.partial(delta_kernel, heads),
        grid=(seqs,),
        out_shape=(
            jax.ShapeDtypeStruct((seqs, heads * size), jnp.bfloat16),
            jax.ShapeDtypeStruct(state.shape, state.dtype),
        ),
        in_specs=[
            scalars,
            scalars,
            scalars,
            own(*x.shape[1:]),
            pl.BlockSpec((1, size), lambda s: (0, 0)),
            own(heads, size, size),
        ],
        out_specs=(
            pl.BlockSpec((seqs, heads * size), lambda s: (0, 0)),
            own(heads, size, size),
        ),
        scratch_shapes=[
            pltpu.VMEM((size, 4 * heads), jnp.float32),
            pltpu.VMEM((seqs * heads, size), jnp.float32),
        ],
        compiler_params=pltpu.CompilerParams(dimension_semantics=("arbitrary",)),
        name="delta",
    )(rate, bias, rates, x, gain.reshape(1, size), state)


def body(
    tokens,
    mix_gain,
    w_query,
    w_key,
    w_value,
    w_zgate,
    w_beta,
    w_decay,
    decay_rate,
    decay_bias,
    head_gain,
    state,
    w_out,
    moe_gain,
    dense_mix,
    dense_gate,
    dense_up,
    dense_down,
    expert_gate,
    expert_up,
    expert_down,
    expert_ids,
    route_weight,
):
    count = lax.axis_size("ep")
    own_rows, width = tokens.shape
    seqs, heads, size, _ = state.shape
    total = 2 * count
    narrow, full = jnp.bfloat16, jnp.float32
    turned = [
        w.transpose(1, 2, 0).reshape(-1, width) for w in (w_query, w_key, w_value, w_zgate)
    ]
    wide = 4 * turned[0].shape[0]
    swapped, rates = comm_call(
        functools.partial(project_kernel, count),
        1,
        (
            jax.ShapeDtypeStruct((count, seqs, wide), narrow),
            jax.ShapeDtypeStruct((seqs, 2 * heads), full),
        ),
        [tokens, mix_gain.reshape(1, width)] + turned + [w_beta.T, w_decay.T],
        [
            VMEM((own_rows, width), narrow),
            VMEM((total, own_rows, width), narrow),
            VMEM((count, seqs, wide), narrow),
        ]
        + sems(copies_of(count, True))
        + sems(count),
    )
    x = swapped.astype(full).transpose(1, 0, 2)
    gated, new_state = delta(decay_rate, decay_bias, rates, x, head_gain, state)
    resid, moe_all = comm_call(
        functools.partial(mix_kernel, count),
        2,
        (
            jax.ShapeDtypeStruct((own_rows, width), full),
            jax.ShapeDtypeStruct((total, own_rows, width), narrow),
        ),
        [gated, w_out, tokens, moe_gain.reshape(1, width)],
        [
            VMEM((count, seqs, heads * size), narrow),
            VMEM((total, own_rows, w_out.shape[1]), narrow),
            VMEM((total, own_rows, w_out.shape[1]), narrow),
            VMEM((own_rows, width), narrow),
        ]
        + sems(copies_of(count, False))
        + sems(total)
        + sems(copies_of(count, True)),
    )
    depth, side = grid_of(count)
    copies = count + (side - 1) * side * depth + (side - 1) * depth + depth - 1
    buf = lambda n: VMEM((n, own_rows, width), narrow)
    layer_out = comm_call(
        functools.partial(moe_kernel, count),
        3,
        jax.ShapeDtypeStruct((own_rows, width), narrow),
        [
            moe_all,
            resid,
            dense_mix.astype(full).reshape(1, width),
            dense_gate,
            dense_up,
            dense_down,
            expert_gate[0],
            expert_up[0],
            expert_down[0],
            expert_ids.T,
            route_weight.T,
        ],
        [buf(total)]
        + [buf(count)] * 3
        + [buf(side * depth)] * 2
        + [buf(depth)] * 2
        + sems(copies),
    )
    return (layer_out, new_state)


def solution(mesh):
    placed = (
        P(("ep", "tp"), None),
        P(),
        P(None, "tp", "ep"),
        P(None, "tp", "ep"),
        P(None, "tp", "ep"),
        P(None, "tp", "ep"),
        P(None, "tp"),
        P(None, "tp"),
        P("tp"),
        P("tp"),
        P(),
        P("ep", "tp", None, None),
        P("tp", "ep"),
        P(),
        P(),
        P(None, ("ep", "tp")),
        P(None, ("ep", "tp")),
        P(("ep", "tp"), None),
        P("ep", None, "tp"),
        P("ep", None, "tp"),
        P("ep", "tp", None),
        P(),
        P(),
    )
    return jax.shard_map(
        body,
        mesh=mesh,
        in_specs=placed,
        out_specs=(P(("ep", "tp"), None), P("ep", "tp", None, None)),
        check_vma=False,
    )
```

profile of v0, /device:TPU:0, one launch (start us, length us, event | category | flops | bytes accessed | tf_op | source)
XLA Modules:
  0.0 107.0 jit_solution(8480468805044729721)
XLA Ops:
  0.6 1.3 %reshape.39 = f32[2048]{0:T(1024)} convert(bf16[2048]{0:T(1024)(128)(2,1)} %param.37) | non-fusion elementwise | flops 2048 | bytes 12288 | tf_op jit(solution)/shard_map/reshape | solution.py:589
  1.9 29.2 %stage_1.1 = (bf16[16,16,256]{2,1,0:T(8,128)(2,1)}, f32[16,16]{1,0:T(8,128)}) custom-call(bf16[8,2048]{1,0:T(8,128)(2,1)} %tokens_ref.3, f32[1,2048]{1,0:T(1,128)} %bitcast.35, bf16[64,2048]{1,0:T(8,128)(2,1)} %bitcast.28, bf16[64,2048]{1,0:T(8,128)(2,1)} %bitcast.29, bf16[64,2048]{1,0:T(8,128)(2,1)} %bitcast.30, bf16[64,2048]{1,0:T(8,128)(2,1)} %bitcast.31, ...), custom_call_target="tpu_custom_call" | custom-call | tf_op jit(solution)/shard_map/stage_1/pallas_call | solution.py:238
  31.1 1.6 %convert_bitcast_fusion.x_ref = f32[16,16,256]{2,1,0:T(8,128)} fusion(bf16[16,16,256]{2,1,0:T(8,128)(2,1)} %get-tuple-element.9), kind=kLoop, calls=%fused_computation | loop fusion | flops 65536 | bytes 393216 | tf_op jit(solution)/shard_map/transpose | solution.py:559
  32.8 16.8 %delta.1 = (bf16[16,1024]{1,0:T(8,128)(2,1)}, f32[16,8,128,128]{3,2,1,0:T(8,128)}) custom-call(f32[8]{0:T(128)} %rate_ref.1, f32[8]{0:T(128)} %bias_ref.1, f32[16,16]{1,0:T(8,128)} %get-tuple-element.8.rates_ref, f32[16,16,256]{2,1,0:T(8,128)} %convert_bitcast_fusion.x_ref, f32[1,128]{1,0:T(1,128)} %bitcast.39, f32[16,8,128,128]{3,2,1,0:T(8,128)} %state_ref.1), custom_call_target="tpu_custom_call" | custom-call | tf_op jit(solution)/shard_map/delta/pallas_call | solution.py:481
  49.5 36.4 %stage_2.1 = (f32[8,2048]{1,0:T(8,128)}, bf16[32,8,2048]{2,1,0:T(8,128)(2,1)}) custom-call(bf16[16,1024]{1,0:T(8,128)(2,1)} %get-tuple-element.10.gated_ref, bf16[1024,128]{1,0:T(8,128)(2,1)} %w_ref.1, bf16[8,2048]{1,0:T(8,128)(2,1)} %tokens_ref.3, f32[1,2048]{1,0:T(1,128)} %bitcast.36), custom_call_target="tpu_custom_call" | custom-call | tf_op jit(solution)/shard_map/stage_2/pallas_call | solution.py:238
  85.9 19.6 %stage_3.1 = bf16[8,2048]{1,0:T(8,128)(2,1)} custom-call(bf16[32,8,2048]{2,1,0:T(8,128)(2,1)} %get-tuple-element.11.rows_ref, f32[8,2048]{1,0:T(8,128)} %get-tuple-element.12.resid_ref, f32[1,2048]{1,0:T(1,128)} %bitcast.34, bf16[2048,128]{1,0:T(8,128)(2,1)} %dg_ref.1, bf16[2048,128]{1,0:T(8,128)(2,1)} %du_ref.1, bf16[128,2048]{1,0:T(8,128)(2,1)} %dd_ref.1, ...), custom_call_target="tpu_custom_call" | custom-call | tf_op jit(solution)/shard_map/stage_3/pallas_call | solution.py:238
  105.6 1.4 %copy.28 = bf16[8,2048]{1,0:T(8,128)(2,1)} copy(bf16[8,2048]{1,0:T(8,128)(2,1)} %stage_3.1) | data formatting | bytes 65536
where the time goes:
time: 108 us; the launch traced here: 107 us
  Pallas kernels  102 us (94%)
  other arithmetic  2.92 us (3%)
  local copies, waits for them, and re-layouts  1.38 us (1%)
    pallas_call x3, Pallas kernels, comm_call(): pl.pallas_call(kernel, out_shape=out_shape, in_specs=[spec] * len(operand...  85.2 us
    pallas_call x1, Pallas kernels, delta(): pl.pallas_call(functools.partial(delta_kernel, heads), grid=(seqs,), out_...  16.8 us

commit v1 on v0

v1 whole, which is shorter than its diff:
```python
import functools

import jax
import jax.numpy as jnp
from jax import lax
from jax.experimental import pallas as pl
from jax.experimental.pallas import tpu as pltpu
from jax.sharding import PartitionSpec as P

EPS = 1e-06
VMEM = pltpu.VMEM
ANY = pl.ANY
MESH = pl.DeviceIdType.MESH
NARROW, FULL = jnp.bfloat16, jnp.float32


def rms_scale(values, gain):
    return values * lax.rsqrt(jnp.mean(values * values, axis=-1, keepdims=True) + EPS) * gain


def silu(v):
    return v / (1.0 + jnp.exp(-v))


def grid_of(count):
    for depth in (4, 2, 1):
        side = int(round((count / depth) ** 0.5))
        if depth * side * side == count:
            return depth, side
    return count, 1


def place_of(count, ep, t):
    depth, side = grid_of(count)
    z = ep // (side * side)
    y = (ep // side) % side
    x = ep % side
    a = x * (1 - t) + y * t
    b = y * (1 - t) + x * t
    return z, b, a


def place(count):
    depth, side = grid_of(count)
    t = lax.axis_index("tp")
    z, b, a = place_of(count, lax.axis_index("ep"), t)
    return depth, side, t, z, b, a


def ep_of(side, t, z, b, a):
    y = b * (1 - t) + a * t
    x = a * (1 - t) + b * t
    return (z * side + y) * side + x


def slot_of(depth, side, z, b, a):
    return (a * side + b) * depth + z


def flip(v, i):
    out = v
    bit = 1
    while bit <= i:
        if i & bit:
            out = out + bit - 2 * bit * ((v // bit) % 2)
        bit *= 2
    return out


def other_core():
    return (lax.axis_index("ep"), 1 - lax.axis_index("tp"))


def near(count):
    depth, side, t, z, b, a = place(count)
    steps = [(flip(z, i), b, a) for i in range(1, depth)]
    steps += [(z, flip(b, i), a) for i in range(1, side)]
    steps += [(z, b, flip(a, i)) for i in range(1, side)]
    return [(ep_of(side, t, *c), t) for c in steps]


def greet(devices):
    barrier = pltpu.get_barrier_semaphore()
    for device in devices:
        pl.semaphore_signal(barrier, inc=1, device_id=device, device_id_type=MESH)
    return len(devices)


def greet_all(count):
    barrier = pltpu.get_barrier_semaphore()
    me = lax.axis_index("ep") * 2 + lax.axis_index("tp")

    def hello(i, carry):
        other = lax.rem(me + i, 2 * count)
        pl.semaphore_signal(
            barrier, inc=1, device_id=(other // 2, other % 2), device_id_type=MESH
        )
        return carry

    lax.fori_loop(1, count * 2, hello, 0)
    return 2 * count - 1


def remote(src, dst, send_sem, recv_sem, device):
    return pltpu.make_async_remote_copy(
        src_ref=src,
        dst_ref=dst,
        send_sem=send_sem,
        recv_sem=recv_sem,
        device_id=device,
        device_id_type=MESH,
    )


def gather(count, pieces, send_sem, recv_sem):
    depth, side, t, z, b, a = place(count)
    number = [0]
    started = []
    arrivals = {}
    peers = {
        "z": [(i, 0, 0) for i in range(1, depth)],
        "b": [(0, i, 0) for i in range(1, side)],
        "a": [(0, 0, i) for i in range(1, side)],
    }
    nothing = (0, 0, 0)
    plus = lambda u, v: tuple(i ^ j for i, j in zip(u, v))

    def at(offset):
        dz, db, da = offset
        return flip(z, dz), flip(b, db), flip(a, da)

    def relay(p, offset, legs):
        source, view, _, _ = pieces[p]
        spot = view(*at(offset))
        for leg in legs:
            for step in peers[leg]:
                n = number[0]
                number[0] += 1
                copy = remote(
                    source if offset == nothing and source is not None else spot,
                    spot,
                    send_sem.at[n],
                    recv_sem.at[n],
                    (ep_of(side, t, *at(step)), t),
                )
                copy.start()
                started.append(copy)
                arrivals[p, leg, plus(offset, step)] = copy

    for p, (_, _, order, arrival) in enumerate(pieces):
        if arrival is not None:
            arrival()
        relay(p, nothing, order)
    for i in range(max(depth, side) - 1):
        for p, (_, _, order, _) in enumerate(pieces):
            if i < len(peers[order[0]]):
                offset = peers[order[0]][i]
                arrivals[p, order[0], offset].wait_recv()
                relay(p, offset, order[1:])
    for p, (_, _, order, _) in enumerate(pieces):
        for first in [nothing] + peers[order[0]]:
            for second in peers[order[1]]:
                offset = plus(first, second)
                arrivals[p, order[1], offset].wait_recv()
                relay(p, offset, order[2:])
    for p, (_, _, order, _) in enumerate(pieces):
        for first in [nothing] + peers[order[0]]:
            for second in [nothing] + peers[order[1]]:
                for third in peers[order[2]]:
                    arrivals[p, order[2], plus(plus(first, second), third)].wait_recv()

    def finish():
        for copy in started:
            copy.wait_send()

    return finish


def contract(left, right):
    return lax.dot_general(left, right, (((1,), (1,)), ((), ())), preferred_element_type=FULL)


def flat_rows(ref):
    blocks, rows, width = ref.shape
    return ref[...].astype(FULL).reshape(blocks * rows, width)


def project_kernel(
    count,
    tokens_ref,
    gain_ref,
    wq_ref,
    wk_ref,
    wv_ref,
    wz_ref,
    beta_ref,
    decay_ref,
    rate_ref,
    bias_ref,
    out_ref,
    columns_ref,
    rows,
    pair,
    normed,
    weights,
    blocks,
    landed,
    flat,
    turned,
    load_sem,
    core_send,
    core_recv,
    send_sem,
    recv_sem,
    send_sem2,
    recv_sem2,
):
    ep = lax.axis_index("ep")
    depth, side, t, z, b, a = place(count)
    partner = other_core()
    per = wq_ref.shape[0]
    heads = beta_ref.shape[0]
    own_rows, width = tokens_ref.shape
    seqs = 2 * own_rows
    total = count * own_rows
    wide = 4 * per
    part = per // heads
    loads = []
    for p, w_ref in enumerate((wq_ref, wk_ref, wv_ref, wz_ref)):
        copy = pltpu.make_async_copy(
            w_ref, weights.at[t, pl.ds(p * per, per)], load_sem.at[p]
        )
        copy.start()
        loads.append(copy)
    expected = greet_all(count)
    my_slot = slot_of(depth, side, z, b, a)
    rows[my_slot] = tokens_ref[...]
    pair[t] = tokens_ref[...]
    source = lax.broadcasted_iota(jnp.int32, (wide, wide), 0)
    target = lax.broadcasted_iota(jnp.int32, (wide, wide), 1)
    inner = source % per
    spot = inner % part * (4 * heads) + source // per * heads + inner // part
    order = jnp.where(target == spot, 1.0, 0.0).astype(NARROW)
    pl.semaphore_wait(pltpu.get_barrier_semaphore(), expected)
    crossed = [remote(tokens_ref, pair.at[t], core_send.at[4], core_recv.at[4], partner)]
    for p, w_ref in enumerate((wq_ref, wk_ref, wv_ref, wz_ref)):
        crossed.append(
            remote(
                w_ref,
                weights.at[t, pl.ds(p * per, per)],
                core_send.at[p],
                core_recv.at[p],
                partner,
            )
        )
    for copy in crossed:
        copy.start()
    view = lambda z, b, a: rows.at[slot_of(depth, side, z, b, a)]
    finish = gather(count, [(tokens_ref, view, "zba", None)], send_sem, recv_sem)
    gain = gain_ref[...]
    for i in range(0, count, 2):
        two = jnp.concatenate([rows[i].astype(FULL), rows[i + 1].astype(FULL)], axis=0)
        normed[i * own_rows : (i + 2) * own_rows] = rms_scale(two, gain).astype(NARROW)
    for copy in loads:
        copy.wait()
    for copy in crossed:
        copy.wait_recv()
    left = normed[...]
    for h in range(2):
        product = contract(left, weights[h]).astype(NARROW)
        moved = jnp.dot(product, order, preferred_element_type=FULL)
        blocks[h] = moved.reshape(count, own_rows, wide).astype(NARROW)
    me = ep * 2 + t

    def copy_to(i):
        other = lax.rem(me + i, 2 * count)
        oe, ot = other // 2, other % 2
        oz, ob, oa = place_of(count, oe, t)
        return remote(
            blocks.at[ot, slot_of(depth, side, oz, ob, oa)],
            landed.at[ep, t],
            send_sem2.at[i],
            recv_sem2.at[i],
            (oe, ot),
        )

    def start(i, carry):
        copy_to(i).start()
        return carry

    def end(i, carry):
        copy_to(i).wait()
        return carry

    lax.fori_loop(1, 2 * count, start, 0)
    landed[ep, t] = blocks[t, my_slot]
    cols = columns_ref.shape[1]
    if cols % 128 == 0:
        span = pl.ds(pl.multiple_of(ep * cols, 128), cols)
        picked = rows[:, :, span].astype(FULL).reshape(total, cols)
    else:
        line = lax.broadcasted_iota(jnp.int32, (width, cols), 0)
        lane = lax.broadcasted_iota(jnp.int32, (width, cols), 1)
        one = jnp.where(line == lane + ep * cols, 1.0, 0.0).astype(NARROW)
        picked = jnp.dot(flat_rows(rows).astype(NARROW), one, preferred_element_type=FULL)
    columns_ref[...] = picked
    seq = rms_scale(flat_rows(pair), gain).astype(NARROW)
    line = lax.broadcasted_iota(jnp.int32, (heads, heads), 0)
    lane = lax.broadcasted_iota(jnp.int32, (heads, heads), 1)
    tall = lambda v: jnp.sum(jnp.where(line == lane, v, 0.0), axis=1, keepdims=True)
    beta = 1.0 / (1.0 + jnp.exp(-contract(beta_ref[...], seq)))
    pre = contract(decay_ref[...], seq) + tall(bias_ref[...])
    soft = jnp.maximum(pre, 0.0) + jnp.log1p(jnp.exp(-jnp.abs(pre)))
    retain = jnp.exp(-tall(rate_ref[...]) * soft)
    size = out_ref.shape[2]
    for s in range(seqs):
        out_ref[s, 4 * heads : 5 * heads, :] = jnp.broadcast_to(beta[:, s : s + 1], (heads, size))
        out_ref[s, 5 * heads :, :] = jnp.broadcast_to(retain[:, s : s + 1], (heads, size))
    finish()
    for copy in crossed:
        copy.wait_send()
    lax.fori_loop(1, 2 * count, end, 0)
    lanes = 4 * heads
    bunch = 128 // lanes
    arrived = landed[...].astype(FULL).reshape(count * seqs, wide)
    for q in range(flat.shape[0]):
        span = arrived[:, q * 128 : (q + 1) * 128]
        flat[q, :, : span.shape[1]] = span
    for g in range(seqs // bunch):
        each = [
            [flat[q, pl.ds(g * bunch + s, count, stride=seqs), :] for q in range(flat.shape[0])]
            for s in range(bunch)
        ]
        for j in range(part):
            q, i = j // bunch, j % bunch
            piece = [v[q][:, i * lanes : (i + 1) * lanes] for v in each]
            piece = jnp.concatenate(piece, axis=1)
            turned[pl.ds(j, count, stride=part), :] = piece
        lines = silu(jnp.transpose(turned[...])).reshape(bunch, 4, heads, size)
        for s in range(bunch):
            for p in range(4):
                v = lines[s, p]
                if p < 2:
                    v = v * lax.rsqrt(jnp.sum(v * v, axis=-1, keepdims=True) + EPS)
                if p == 0:
                    v = v * size ** (-0.5)
                out_ref[g * bunch + s, p * heads : (p + 1) * heads, :] = v


def sems(n):
    return [pltpu.SemaphoreType.DMA((n,)), pltpu.SemaphoreType.DMA((n,))]


def comm_call(kernel, number, out_shape, operands, scratch):
    spec = pl.BlockSpec(memory_space=VMEM)
    return pl.pallas_call(
        kernel,
        out_shape=out_shape,
        in_specs=[pl.BlockSpec(memory_space=ANY) if away else spec for _, away in operands],
        out_specs=jax.tree.map(lambda _: spec, out_shape),
        scratch_shapes=scratch,
        compiler_params=pltpu.CompilerParams(
            collective_id=number, has_side_effects=True, vmem_limit_bytes=60 * 1024 * 1024
        ),
        name=f"stage_{number}",
    )(*[v for v, _ in operands])


def expert_kernel(
    count,
    gated_ref,
    columns_ref,
    gains_ref,
    mix_ref,
    ids_ref,
    route_ref,
    w_ref,
    dg_ref,
    du_ref,
    dd_ref,
    eg_ref,
    eu_ref,
    ed_ref,
    out_ref,
    rows,
    wo,
    dg,
    du,
    dd,
    eg,
    eu,
    ed,
    own,
    every,
    part,
    a_buf,
    sum1,
    b_buf,
    sum2,
    z_buf,
    load_sem,
    core_send,
    core_recv,
    send_sem,
    recv_sem,
    send_sem2,
    recv_sem2,
    send_sem3,
    recv_sem3,
):
    ep = lax.axis_index("ep")
    depth, side, t, z, b, a = place(count)
    partner = other_core()
    own_rows = gated_ref.shape[1]
    half = gated_ref.shape[2]
    total = count * own_rows
    cols = columns_ref.shape[1]
    shards = (w_ref, dg_ref, du_ref, eg_ref, eu_ref, dd_ref, ed_ref)
    places = (wo, dg, du, eg, eu, dd, ed)
    loads = []
    for i, (src, dst) in enumerate(zip(shards, places)):
        copy = pltpu.make_async_copy(src, dst.at[t], load_sem.at[i])
        copy.start()
        loads.append(copy)
    expected = greet([partner] + near(count))
    my_slot = slot_of(depth, side, z, b, a)
    mine = pl.ds(pl.multiple_of(t * half, half), half)
    others = pl.ds(pl.multiple_of((1 - t) * half, half), half)
    rows[my_slot, :, mine] = gated_ref[t]
    weight = jnp.sum(jnp.where(ids_ref[...] == ep, route_ref[...], 0.0), axis=0, keepdims=True)
    tokens = weight.shape[1]
    line = lax.broadcasted_iota(jnp.int32, (total, tokens), 0)
    lane = lax.broadcasted_iota(jnp.int32, (total, tokens), 1)
    place_id = line // own_rows
    chip = ep_of(
        side, t, place_id % depth, (place_id // depth) % side, place_id // (depth * side)
    )
    token = chip * (2 * own_rows) + t * own_rows + line % own_rows
    weight = jnp.sum(jnp.where(token == lane, weight, 0.0), axis=1, keepdims=True)
    pl.semaphore_wait(pltpu.get_barrier_semaphore(), expected)
    there = slot_of(depth, side, *place_of(count, ep, 1 - t))
    swap = remote(
        gated_ref.at[1 - t],
        rows.at[there, :, mine],
        core_send.at[7],
        core_recv.at[7],
        partner,
    )
    swap.start()
    crossed = []
    for i, (src, dst) in enumerate(zip(shards, places)):
        crossed.append(remote(src, dst.at[t], core_send.at[i], core_recv.at[i], partner))

    def arrive():
        swap.wait_recv()
        for copy in crossed:
            copy.start()

    view = lambda span: lambda z, b, a: rows.at[slot_of(depth, side, z, b, a), :, span]
    finish1 = gather(
        count,
        [(gated_ref.at[t], view(mine), "zba", None), (None, view(others), "zba", arrive)],
        send_sem,
        recv_sem,
    )
    loads[0].wait()
    crossed[0].wait_recv()
    flat = flat_rows(rows).astype(NARROW)
    product = jnp.dot(flat[:, :half], wo[0], preferred_element_type=FULL)
    product = product + jnp.dot(flat[:, half:], wo[1], preferred_element_type=FULL)
    resid = columns_ref[...] + product
    own[...] = (resid * gains_ref[pl.ds(ep, 1), :]).astype(NARROW)
    every[ep] = own[...]
    finish2 = gather(
        count,
        [(own, lambda z, b, a: every.at[ep_of(side, t, z, b, a)], "zba", None)],
        send_sem2,
        recv_sem2,
    )
    mixes = mix_ref[...].astype(FULL)
    inverse = 1.0 / gains_ref[...]
    squares = jnp.zeros((total, cols), FULL)
    mixed = jnp.zeros((total, cols), FULL)
    for e in range(count):
        v = every[e].astype(FULL)
        r = v * inverse[e : e + 1]
        squares = squares + r * r
        mixed = mixed + v * mixes[e : e + 1]
    width = count * cols
    scale = lax.rsqrt(jnp.sum(squares, axis=1, keepdims=True) * (1.0 / width) + EPS)
    mixed = scale * jnp.sum(mixed, axis=1, keepdims=True)
    mixed = 1.0 / (1.0 + jnp.exp(-mixed))
    left = jnp.concatenate([every[e] for e in range(count)], axis=1)
    for i in (1, 2, 3, 4):
        loads[i].wait()
        crossed[i].wait_recv()

    def hidden(gate, up, factor):
        gate = scale * jnp.dot(left, gate, preferred_element_type=FULL)
        up = scale * jnp.dot(left, up, preferred_element_type=FULL)
        return (silu(gate) * up * factor).astype(NARROW)

    join = lambda ref: jnp.concatenate([ref[0], ref[1]], axis=1)
    acts = [hidden(join(dg), join(du), mixed)]
    acts += [hidden(eg[h], eu[h], weight) for h in range(2)]
    for i in (5, 6):
        loads[i].wait()
        crossed[i].wait_recv()
    chunks, step = part.shape[0], part.shape[-1]
    ffd = dd.shape[1]
    number = [0]
    started = []

    def send(src, dst, device):
        n = number[0]
        number[0] += 1
        copy = remote(src, dst, send_sem3.at[n], recv_sem3.at[n], device)
        copy.start()
        started.append(copy)
        return copy

    device_of = lambda z, b, a: (ep_of(side, t, z, b, a), t)
    wait1, wait2, wait3 = {}, {}, {}

    def down(c):
        span = slice(c * step, (c + 1) * step)
        term = jnp.dot(acts[0][:, :ffd], dd[0, :, span], preferred_element_type=FULL)
        term = term + jnp.dot(acts[0][:, ffd:], dd[1, :, span], preferred_element_type=FULL)
        for h in range(2):
            term = term + jnp.dot(acts[1 + h], ed[h, :, span], preferred_element_type=FULL)
        part[c] = term.reshape(part.shape[1:]).astype(NARROW)
        for i in range(1, side):
            far = flip(a, i)
            wait1[c, i] = send(part.at[c, far], a_buf.at[c, i - 1], device_of(z, b, far))

    def second(c):
        sums = part[c, a].astype(FULL)
        for i in range(1, side):
            wait1[c, i].wait_recv()
            sums = sums + a_buf[c, i - 1].astype(FULL)
        sum1[c] = sums.astype(NARROW)
        for i in range(1, side):
            far = flip(b, i)
            wait2[c, i] = send(sum1.at[c, far], b_buf.at[c, i - 1], device_of(z, far, a))

    def third(c):
        sums = sum1[c, b].astype(FULL)
        for i in range(1, side):
            wait2[c, i].wait_recv()
            sums = sums + b_buf[c, i - 1].astype(FULL)
        sum2[c] = sums.astype(NARROW)
        for i in range(1, depth):
            far = flip(z, i)
            wait3[c, i] = send(sum2.at[c, far], z_buf.at[c, i - 1], device_of(far, b, a))

    for c in range(chunks):
        down(c)
    for c in range(chunks):
        second(c)
    line = lax.broadcasted_iota(jnp.int32, (own_rows, total), 0)
    lane = lax.broadcasted_iota(jnp.int32, (own_rows, total), 1)
    pick = jnp.where(lane == line + my_slot * own_rows, 1.0, 0.0).astype(NARROW)
    back = [
        jnp.dot(pick, every[e], preferred_element_type=FULL) * inverse[e : e + 1]
        for e in range(count)
    ]
    resid = jnp.concatenate(back, axis=1)
    for c in range(chunks):
        third(c)
    for c in range(chunks):
        sums = resid[:, c * step : (c + 1) * step] + sum2[c, z].astype(FULL)
        for i in range(1, depth):
            wait3[c, i].wait_recv()
            sums = sums + z_buf[c, i - 1].astype(FULL)
        out_ref[:, c * step : (c + 1) * step] = sums.astype(out_ref.dtype)
    finish1()
    finish2()
    swap.wait_send()
    for copy in crossed + started:
        copy.wait_send()


def delta_kernel(heads, r_ref, gain_ref, state_ref, gated_ref, new_ref, acc):
    step = pl.program_id(0)
    bunch = state_ref.shape[0]
    size = state_ref.shape[2]
    for s in range(bunch):
        query = r_ref[s, 0:heads]
        key = r_ref[s, heads : 2 * heads]
        value = r_ref[s, 2 * heads : 3 * heads]
        gate = r_ref[s, 3 * heads : 4 * heads]
        beta = r_ref[s, 4 * heads : 5 * heads]
        keep = r_ref[s, 5 * heads : 6 * heads]
        both = r_ref[s, 0 : 2 * heads]
        high = both.astype(NARROW)
        low = (both - high.astype(FULL)).astype(NARROW)
        left = jnp.concatenate([high, low], axis=0)
        line = lax.broadcasted_iota(jnp.int32, (2 * heads, size), 0) % heads
        reads = jnp.zeros((2 * heads, size), FULL)
        for h in range(heads):
            got = jnp.dot(left, state_ref[s, h].astype(NARROW), preferred_element_type=FULL)
            reads = jnp.where(line == h, got[: 2 * heads] + got[2 * heads :], reads)
        recalled = reads[heads:]
        write = beta * (value - keep * recalled)
        readout = keep * reads[:heads] + jnp.sum(key * query, axis=1, keepdims=True) * write
        gated = rms_scale(readout, gain_ref[...]) * gate
        first = pl.multiple_of((step * bunch + s) * heads, heads)
        acc[pl.ds(first, heads), :] = gated
        split = lambda v: (
            v.astype(NARROW).astype(FULL),
            (v - v.astype(NARROW).astype(FULL)),
        )
        k_high, k_low = split(key)
        w_high, w_low = split(write)
        none = jnp.zeros_like(key)
        tall = jnp.transpose(jnp.concatenate([k_high, k_high, k_low, none], axis=0)).astype(NARROW)
        across = jnp.concatenate([w_high, w_low, w_high, none], axis=0)
        row = lax.broadcasted_iota(jnp.int32, across.shape, 0) % heads
        for h in range(0, heads, 2):
            two = jnp.concatenate(
                [jnp.where(row == h + i, across, 0.0) for i in range(2)], axis=1
            ).astype(NARROW)
            outer = jnp.dot(tall, two, preferred_element_type=FULL)
            for i in range(2):
                new_ref[s, h + i] = (
                    keep[h + i : h + i + 1] * state_ref[s, h + i]
                    + outer[:, i * size : (i + 1) * size]
                )

    @pl.when(step == pl.num_programs(0) - 1)
    def _():
        halves, rows = gated_ref.shape[:2]
        for i in range(halves):
            for h in range(heads):
                piece = acc[pl.ds(i * rows * heads + h, rows, stride=heads), :]
                gated_ref[i, :, h * size : (h + 1) * size] = piece.astype(gated_ref.dtype)


def delta(ready, gain, state):
    seqs, heads, size, _ = state.shape
    bunch = 2
    own = lambda *shape: pl.BlockSpec((bunch,) + shape, lambda s: (s,) + (0,) * len(shape))
    return pl.pallas_call(
        functools.partial(delta_kernel, heads),
        grid=(seqs // bunch,),
        out_shape=(
            jax.ShapeDtypeStruct((2, seqs // 2, heads * size), NARROW),
            jax.ShapeDtypeStruct(state.shape, state.dtype),
        ),
        in_specs=[
            own(*ready.shape[1:]),
            pl.BlockSpec((1, size), lambda s: (0, 0)),
            own(heads, size, size),
        ],
        out_specs=(
            pl.BlockSpec((2, seqs // 2, heads * size), lambda s: (0, 0, 0)),
            own(heads, size, size),
        ),
        scratch_shapes=[VMEM((seqs * heads, size), FULL)],
        compiler_params=pltpu.CompilerParams(dimension_semantics=("arbitrary",)),
        name="delta",
    )(ready, gain.reshape(1, size), state)


def body(
    tokens,
    mix_gain,
    w_query,
    w_key,
    w_value,
    w_zgate,
    w_beta,
    w_decay,
    decay_rate,
    decay_bias,
    head_gain,
    state,
    w_out,
    moe_gain,
    dense_mix,
    dense_gate,
    dense_up,
    dense_down,
    expert_gate,
    expert_up,
    expert_down,
    expert_ids,
    route_weight,
):
    count = lax.axis_size("ep")
    own_rows, width = tokens.shape
    seqs, heads, size, _ = state.shape
    depth, side = grid_of(count)
    total = count * own_rows
    turned = [
        w.transpose(1, 2, 0).reshape(-1, width) for w in (w_query, w_key, w_value, w_zgate)
    ]
    wide = 4 * turned[0].shape[0]
    cols = w_out.shape[1]
    ready, columns = comm_call(
        functools.partial(project_kernel, count),
        1,
        (
            jax.ShapeDtypeStruct((seqs, 6 * heads, size), FULL),
            jax.ShapeDtypeStruct((total, cols), FULL),
        ),
        [(tokens, False), (mix_gain.reshape(1, width), False)]
        + [(w, True) for w in turned]
        + [(w_beta.T, False), (w_decay.T, False)]
        + [(decay_rate.reshape(1, heads), False), (decay_bias.reshape(1, heads), False)],
        [
            VMEM((count, own_rows, width), NARROW),
            VMEM((2, own_rows, width), NARROW),
            VMEM((total, width), NARROW),
            VMEM((2, wide, width), NARROW),
            VMEM((2, count, own_rows, wide), NARROW),
            VMEM((count, 2, own_rows, wide), NARROW),
            VMEM((-(-wide // 128), count * seqs, 128), FULL),
            VMEM((size, 128), FULL),
            pltpu.SemaphoreType.DMA((4,)),
        ]
        + sems(5)
        + sems(count - 1)
        + sems(2 * count),
    )
    gated, new_state = delta(ready, head_gain, state)
    chunks = 4
    step = width // chunks
    shard = lambda w: VMEM((2,) + w.shape, NARROW)
    held = (w_out, dense_gate, dense_up, dense_down, expert_gate[0], expert_up[0], expert_down[0])
    layer_out = comm_call(
        functools.partial(expert_kernel, count),
        2,
        jax.ShapeDtypeStruct((own_rows, width), NARROW),
        [
            (gated, False),
            (columns, False),
            (moe_gain.reshape(count, cols), False),
            (dense_mix.reshape(count, cols), False),
            (expert_ids.T, False),
            (route_weight.T, False),
        ]
        + [(w, True) for w in held],
        [VMEM((count, own_rows, width), NARROW)]
        + [shard(w) for w in held]
        + [
            VMEM((total, cols), NARROW),
            VMEM((count, total, cols), NARROW),
            VMEM((chunks, side, side, depth, own_rows, step), NARROW),
            VMEM((chunks, max(side - 1, 1), side, depth, own_rows, step), NARROW),
            VMEM((chunks, side, depth, own_rows, step), NARROW),
            VMEM((chunks, max(side - 1, 1), depth, own_rows, step), NARROW),
            VMEM((chunks, depth, own_rows, step), NARROW),
            VMEM((chunks, max(depth - 1, 1), own_rows, step), NARROW),
            pltpu.SemaphoreType.DMA((7,)),
        ]
        + sems(8)
        + sems(2 * (count - 1))
        + sems(count - 1)
        + sems(chunks * (2 * (side - 1) + depth - 1)),
    )
    return (layer_out, new_state)


def solution(mesh):
    placed = (
        P(("ep", "tp"), None),
        P(),
        P(None, "tp", "ep"),
        P(None, "tp", "ep"),
        P(None, "tp", "ep"),
        P(None, "tp", "ep"),
        P(None, "tp"),
        P(None, "tp"),
        P("tp"),
        P("tp"),
        P(),
        P("ep", "tp", None, None),
        P("tp", "ep"),
        P(),
        P(),
        P(None, ("ep", "tp")),
        P(None, ("ep", "tp")),
        P(("ep", "tp"), None),
        P("ep", None, "tp"),
        P("ep", None, "tp"),
        P("ep", "tp", None),
        P(),
        P(),
    )
    return jax.shard_map(
        body,
        mesh=mesh,
        in_specs=placed,
        out_specs=(P(("ep", "tp"), None), P("ep", "tp", None, None)),
        check_vma=False,
    )
```

time: 108 us -> 82.3 us (0.76)
  Pallas kernels: 102 us -> 79.7 us
  other arithmetic: 2.92 us -> 0 us
    pallas_call x4 -> x3, Pallas kernels: 102 us -> 79.7 us  [the longest x2 69 us: comm_call(): pl.pallas_call(kernel, out_shape=out_shape, in_specs=[pl.BlockSpec(memory...]
    transpose x1 -> x0, other arithmetic: 1.64 us -> none  [body(): x = swapped.astype(full).transpose(1, 0, 2)]
    reshape x1 -> x0, other arithmetic: 1.28 us -> none  [body(): dense_mix.astype(full).reshape(1, width)]
where the time goes in v1:
time: 82.3 us; the launch traced here: 81.8 us
  Pallas kernels  79.7 us (97%)
  local copies, waits for them, and re-layouts  1.38 us (2%)
    pallas_call x2, Pallas kernels, comm_call(): pl.pallas_call(kernel, out_shape=out_shape, in_specs=[pl.BlockSpec(memory...  69 us
    pallas_call x1, Pallas kernels, delta(): pl.pallas_call(functools.partial(delta_kernel, heads), grid=(seqs // bunc...  10.7 us

profile of v1, /device:TPU:0, one launch (start us, length us, event | category | flops | bytes accessed | tf_op | source)
XLA Modules:
  0.0 81.8 jit_solution(7493726663741311357)
XLA Ops:
  0.6 27.8 %stage_1.1 = (f32[16,48,128]{2,1,0:T(8,128)}, f32[128,128]{1,0:T(8,128)}) custom-call(bf16[8,2048]{1,0:T(8,128)(2,1)} %tokens_ref.1, f32[1,2048]{1,0:T(1,128)} %bitcast.34, bf16[64,2048]{1,0:T(8,128)(2,1)} %bitcast.28, bf16[64,2048]{1,0:T(8,128)(2,1)} %bitcast.29, bf16[64,2048]{1,0:T(8,128)(2,1)} %bitcast.30, bf16[64,2048]{1,0:T(8,128)(2,1)} %bitcast.31, ...), custom_call_target="tpu_custom_call" | custom-call | tf_op jit(solution)/shard_map/stage_1/pallas_call | solution.py:356
  28.4 10.7 %delta.1 = (bf16[2,8,1024]{2,1,0:T(8,128)(2,1)}, f32[16,8,128,128]{3,2,1,0:T(8,128)}) custom-call(f32[16,48,128]{2,1,0:T(8,128)} %get-tuple-element.6.r_ref, f32[1,128]{1,0:T(1,128)} %bitcast.41, f32[16,8,128,128]{3,2,1,0:T(8,128)} %state_ref.1), custom_call_target="tpu_custom_call" | custom-call | tf_op jit(solution)/shard_map/delta/pallas_call | solution.py:643
  39.1 41.2 %stage_2.1 = bf16[8,2048]{1,0:T(8,128)(2,1)} custom-call(bf16[2,8,1024]{2,1,0:T(8,128)(2,1)} %get-tuple-element.7.gated_ref, f32[128,128]{1,0:T(8,128)} %get-tuple-element.8.columns_ref, f32[16,128]{1,0:T(8,128)} %bitcast.35, bf16[16,128]{1,0:T(8,128)(2,1)} %bitcast.36, s32[4,256]{1,0:T(4,128)} %bitcast.37, f32[4,256]{1,0:T(4,128)} %bitcast.38, ...), custom_call_target="tpu_custom_call" | custom-call | tf_op jit(solution)/shard_map/stage_2/pallas_call | solution.py:356
  80.4 1.4 %copy.26 = bf16[8,2048]{1,0:T(8,128)(2,1)} copy(bf16[8,2048]{1,0:T(8,128)(2,1)} %stage_2.1) | data formatting | bytes 65536

commit v2 on v1

v2 whole, which is shorter than its diff:
```python
import functools
import types

import jax
import jax.numpy as jnp
from jax import lax
from jax.experimental import pallas as pl
from jax.experimental.pallas import tpu as pltpu
from jax.sharding import PartitionSpec as P

EPS = 1e-06
VMEM = pltpu.VMEM
HBM = pltpu.HBM
MESH = pl.DeviceIdType.MESH
NARROW, FULL = jnp.bfloat16, jnp.float32


def rms_scale(values, gain):
    return values * lax.rsqrt(jnp.mean(values * values, axis=-1, keepdims=True) + EPS) * gain


def silu(v):
    return v / (1.0 + jnp.exp(-v))


def grid_of(count):
    for depth in (4, 2, 1):
        side = int(round((count / depth) ** 0.5))
        if depth * side * side == count:
            return depth, side
    return count, 1


def place_of(count, ep, t):
    depth, side = grid_of(count)
    z = ep // (side * side)
    y = (ep // side) % side
    x = ep % side
    a = x * (1 - t) + y * t
    b = y * (1 - t) + x * t
    return z, b, a


def place(count):
    depth, side = grid_of(count)
    t = lax.axis_index("tp")
    z, b, a = place_of(count, lax.axis_index("ep"), t)
    return depth, side, t, z, b, a


def ep_of(side, t, z, b, a):
    y = b * (1 - t) + a * t
    x = a * (1 - t) + b * t
    return (z * side + y) * side + x


def slot_of(depth, side, z, b, a):
    return (z * side + a) * side + b


def flip(v, i):
    out = v
    bit = 1
    while bit <= i:
        if i & bit:
            out = out + bit - 2 * bit * ((v // bit) % 2)
        bit *= 2
    return out


def other_core():
    return (lax.axis_index("ep"), 1 - lax.axis_index("tp"))


def peers_of(count):
    depth, side = grid_of(count)
    plane = [(0, j, i) for j in range(side) for i in range(side)][1:]
    plane.sort(key=lambda o: -(o[1] > 0) - (o[2] > 0))
    return [(i, 0, 0) for i in range(1, depth)], plane


def at(here, offset):
    return tuple(flip(v, i) for v, i in zip(here, offset))


def remote(src, dst, sems, n, device):
    return pltpu.make_async_remote_copy(
        src_ref=src,
        dst_ref=dst,
        send_sem=sems[0].at[n],
        recv_sem=sems[1].at[n],
        device_id=device,
        device_id_type=MESH,
    )


def gather(count, pieces, sems, landed=None, then=None):
    depth, side, t, *here = place(count)
    lines, plane = peers_of(count)
    started = []
    arrivals = {}
    nothing = (0, 0, 0)
    plus = lambda u, v: tuple(i ^ j for i, j in zip(u, v))

    def spread(p, offset, steps):
        source, view, _ = pieces[p]
        spot = view(*at(here, offset))
        if offset == nothing and source is not None:
            source_ref = source
        else:
            source_ref = spot
        for step in steps:
            device = (ep_of(side, t, *at(here, step)), t)
            copy = remote(source_ref, spot, sems, len(started), device)
            copy.start()
            started.append(copy)
            arrivals[p, plus(offset, step)] = copy

    for p, (_, _, arrival) in enumerate(pieces):
        if arrival is not None:
            arrival()
        spread(p, nothing, plane + lines)
    if then is not None:
        then()
    for offset in lines:
        for p in range(len(pieces)):
            arrivals[p, offset].wait_recv()
            spread(p, offset, plane)
    for offset in [nothing] + lines:
        for p in range(len(pieces)):
            for step in plane:
                arrivals[p, plus(offset, step)].wait_recv()
        if landed is not None:
            landed(offset[0])

    def finish():
        for copy in started:
            copy.wait_send()

    return finish


def contract(left, right):
    return lax.dot_general(left, right, (((1,), (1,)), ((), ())), preferred_element_type=FULL)


def dot(left, right):
    return jnp.dot(left, right, preferred_element_type=FULL)


def flat_rows(ref):
    blocks, rows, width = ref.shape
    return ref[...].astype(FULL).reshape(blocks * rows, width)


def grid_ids(*shape):
    return tuple(lax.broadcasted_iota(jnp.int32, shape, i) for i in range(2))


def sigmoid(v):
    return 1.0 / (1.0 + jnp.exp(-v))


def layer_kernel(count, names, pairs, *refs):
    r = types.SimpleNamespace(**dict(zip(names, refs)))
    for name in pairs:
        setattr(r, name, (getattr(r, name + "_send"), getattr(r, name + "_recv")))
    ep = lax.axis_index("ep")
    depth, side, t, *here = place(count)
    z, b, a = here
    lines, plane = peers_of(count)
    partner = (ep, 1 - t)
    own_rows, width = r.tokens.shape
    seqs = 2 * own_rows
    total = count * own_rows
    per = r.wq_hbm.shape[0]
    wide = 4 * per
    heads = r.beta.shape[0]
    part = per // heads
    size = width // (2 * heads)
    half = heads * size
    cols = r.wo.shape[2]
    my_slot = slot_of(depth, side, *here)
    slots = lambda ref: lambda z, b, a: ref.at[slot_of(depth, side, z, b, a)]

    loads = {}

    def load(name, src, dst):
        copy = pltpu.make_async_copy(src, dst, r.load_sem.at[len(loads)])
        copy.start()
        loads[name] = copy

    small = ("tokens", "gain", "beta", "decay", "rate", "bias", "head_gain")
    late = ("moe_gain", "mix", "ids", "route")
    for name in small:
        load(name, getattr(r, name + "_hbm"), getattr(r, name))
    projections = (r.wq_hbm, r.wk_hbm, r.wv_hbm, r.wz_hbm)
    spot_of = lambda p: r.weights.at[t, pl.ds(p * per, per)]
    for p, src in enumerate(projections):
        load(("w", p), src, spot_of(p))
    for s in range(seqs):
        load(("state", s), r.state_hbm.at[s], r.state.at[s])
    for name in late:
        load(name, getattr(r, name + "_hbm"), getattr(r, name))
    shards = ("wo", "dg", "du", "eg", "eu", "dd", "ed")
    for name in shards:
        load(name, getattr(r, name + "_hbm"), getattr(r, name).at[t])

    barrier = pltpu.get_barrier_semaphore()
    devices = [partner] + [(ep_of(side, t, *at(here, o)), t) for o in plane + lines]
    for device in devices:
        pl.semaphore_signal(barrier, inc=1, device_id=device, device_id_type=MESH)
    source, target = grid_ids(wide, wide)
    inner = source % per
    spot = inner % part * (4 * heads) + source // per * heads + inner // part
    order = jnp.where(target == spot, 1.0, 0.0).astype(NARROW)
    loads["tokens"].wait()
    r.rows[my_slot] = r.tokens[...]
    r.pair[t] = r.tokens[...]
    pl.semaphore_wait(barrier, len(devices))

    crossed = {}

    def cross(name, src, dst):
        copy = remote(src, dst, r.core, len(crossed), partner)
        copy.start()
        crossed[name] = copy

    def begin():
        cross("pair", r.tokens, r.pair.at[t])
        for p, src in enumerate(projections):
            cross(("w", p), src, spot_of(p))

    loads["gain"].wait()
    gain = r.gain[...]
    square = side * side

    def normalise(i):
        far = flip(z, i)
        for k in range(0, square, 2):
            first = far * square + k
            two = [r.rows[first + j].astype(FULL) for j in range(2)]
            two = rms_scale(jnp.concatenate(two, axis=0), gain).astype(NARROW)
            start = pl.multiple_of(first * own_rows, 2 * own_rows)
            r.normed[pl.ds(start, 2 * own_rows)] = two

    finish1 = gather(
        count, [(r.tokens, slots(r.rows), None)], r.ring1, normalise, then=begin
    )
    for p in range(4):
        loads["w", p].wait()
        crossed["w", p].wait_recv()
    for name in shards:
        cross(name, getattr(r, name + "_hbm"), getattr(r, name).at[t])
    left = r.normed[...]
    for h in range(2):
        product = contract(left, r.weights[h]).astype(NARROW)
        moved = dot(product, order)
        r.blocks[h] = moved.reshape(count, own_rows, wide).astype(NARROW)

    exchange = []
    for offset in [(i, j, k) for i in range(depth) for j in range(side) for k in range(side)][::-1]:
        z2, b2, a2 = at(here, offset)
        other = ep_of(side, t, z2, b2, a2)
        row = slot_of(depth, side, z2, b2, a2)
        for core in (1 - t, t):
            if offset == (0, 0, 0) and core is t:
                continue
            copy = remote(
                r.blocks.at[core, row], r.landed.at[ep, t], r.swap, len(exchange), (other, core)
            )
            copy.start()
            exchange.append(copy)
    r.landed[ep, t] = r.blocks[t, my_slot]

    if cols % 128 == 0:
        span = pl.ds(pl.multiple_of(ep * cols, 128), cols)
        r.columns[...] = r.rows[:, :, span].astype(FULL).reshape(total, cols)
    else:
        line, lane = grid_ids(width, cols)
        one = jnp.where(line == lane + ep * cols, 1.0, 0.0).astype(NARROW)
        r.columns[...] = dot(flat_rows(r.rows).astype(NARROW), one)
    crossed["pair"].wait_recv()
    for name in small[2:]:
        loads[name].wait()
    seq = rms_scale(flat_rows(r.pair), gain).astype(NARROW)
    line, lane = grid_ids(heads, heads)
    tall = lambda v: jnp.sum(jnp.where(line == lane, v, 0.0), axis=1, keepdims=True)
    beta = sigmoid(contract(r.beta[...], seq))
    pre = contract(r.decay[...], seq) + tall(r.bias[...])
    soft = jnp.maximum(pre, 0.0) + jnp.log1p(jnp.exp(-jnp.abs(pre)))
    retain = jnp.exp(-tall(r.rate[...]) * soft)
    for s in range(seqs):
        r.ready[4, s] = jnp.broadcast_to(beta[:, s : s + 1], (heads, size))
        r.ready[5, s] = jnp.broadcast_to(retain[:, s : s + 1], (heads, size))
    for name in late:
        loads[name].wait()
    weight = jnp.sum(jnp.where(r.ids[...] == ep, r.route[...], 0.0), axis=0, keepdims=True)
    line, lane = grid_ids(total, weight.shape[1])
    place_id = line // own_rows
    chip = ep_of(side, t, place_id // square, place_id % side, (place_id // side) % side)
    token = chip * seqs + t * own_rows + line % own_rows
    weight = jnp.sum(jnp.where(token == lane, weight, 0.0), axis=1, keepdims=True)
    r.weight[...] = jnp.broadcast_to(weight, r.weight.shape)
    r.mixes[...] = r.mix[...].astype(FULL)
    finish1()
    for s in range(seqs):
        loads["state", s].wait()
    for copy in exchange:
        copy.wait()

    lanes = 4 * heads
    bunch = 128 // lanes
    arrived = r.landed[...].astype(FULL).reshape(count * seqs, wide)
    planes = r.flat.shape[0]
    for q in range(planes):
        span = arrived[:, q * 128 : (q + 1) * 128]
        r.flat[q, :, : span.shape[1]] = span
    for g in range(seqs // bunch):
        each = [
            [r.flat[q, pl.ds(g * bunch + s, count, stride=seqs), :] for q in range(planes)]
            for s in range(bunch)
        ]
        for j in range(part):
            q, i = j // bunch, j % bunch
            piece = [v[q][:, i * lanes : (i + 1) * lanes] for v in each]
            r.turned[g, pl.ds(j, count, stride=part), :] = jnp.concatenate(piece, axis=1)
    for g in range(seqs // bunch):
        split = silu(jnp.transpose(r.turned[g])).reshape(bunch, 4, heads, size)
        for p in range(4):
            v = split[:, p]
            if p < 2:
                v = v * lax.rsqrt(jnp.sum(v * v, axis=-1, keepdims=True) + EPS)
            if p == 0:
                v = v * size ** (-0.5)
            r.ready[p, g * bunch : (g + 1) * bunch] = v

    there = slot_of(depth, side, *place_of(count, ep, 1 - t))
    mine = pl.ds(pl.multiple_of(t * half, half), half)
    others = pl.ds(pl.multiple_of((1 - t) * half, half), half)
    head_gain = r.head_gain[...]
    line = lax.broadcasted_iota(jnp.int32, (2 * heads, size), 0) % heads

    def readouts(core):
        first = core * own_rows
        reads = []
        for i in range(own_rows):
            s = first + i
            both = jnp.concatenate([r.ready[0, s], r.ready[1, s]], axis=0)
            high = both.astype(NARROW)
            low = (both - high.astype(FULL)).astype(NARROW)
            pushed = jnp.concatenate([high, low], axis=0)
            kept = jnp.zeros((2 * heads, size), FULL)
            for h in range(heads):
                got = dot(pushed, r.state[s, h].astype(NARROW))
                kept = jnp.where(line == h, got[: 2 * heads] + got[2 * heads :], kept)
            reads.append(kept)
        rows = pl.ds(pl.multiple_of(first, own_rows), own_rows)
        query, key, value, gate, beta, keep = (
            r.ready[p, rows].reshape(own_rows * heads, size) for p in range(6)
        )
        recalled = jnp.concatenate([v[heads:] for v in reads], axis=0)
        asked = jnp.concatenate([v[:heads] for v in reads], axis=0)
        write = beta * (value - keep * recalled)
        readout = keep * asked + jnp.sum(key * query, axis=1, keepdims=True) * write
        r.write[rows] = write.reshape(own_rows, heads, size)
        r.acc[...] = rms_scale(readout, head_gain) * gate
        for h in range(heads):
            piece = r.acc[pl.ds(h, own_rows, stride=heads), :]
            r.gated[core, :, h * size : (h + 1) * size] = piece.astype(NARROW)

    readouts(1 - t)
    swap = remote(r.gated.at[1 - t], r.mixed.at[there, :, mine], r.core, len(crossed), partner)
    swap.start()
    readouts(t)
    r.mixed[my_slot, :, mine] = r.gated[t]

    view = lambda span: lambda z, b, a: r.mixed.at[slot_of(depth, side, z, b, a), :, span]

    groups = seqs // bunch

    def prepare():
        keep = r.ready[5].reshape(seqs * heads, size)
        r.pack[2 * groups] = keep.astype(NARROW)
        r.pack[2 * groups + 1] = (keep - keep.astype(NARROW).astype(FULL)).astype(NARROW)
        none = jnp.zeros((heads, size), FULL)
        high = lambda v: v.astype(NARROW).astype(FULL)
        for g in range(groups):
            tall, across = [], []
            for s in range(g * bunch, (g + 1) * bunch):
                key, write = r.ready[1, s], r.write[s]
                tall += [high(key), high(key), key - high(key), none]
                across += [high(write), write - high(write), high(write), none]
            r.pack[g] = jnp.transpose(jnp.concatenate(tall, axis=0)).astype(NARROW)
            r.pack[groups + g] = jnp.concatenate(across, axis=0).astype(NARROW)

    finish2 = gather(
        count,
        [(r.gated.at[t], view(mine), None), (None, view(others), swap.wait_recv)],
        r.ring2,
        then=prepare,
    )
    loads["wo"].wait()
    crossed["wo"].wait_recv()
    flat = flat_rows(r.mixed).astype(NARROW)
    resid = r.columns[...] + dot(flat[:, :half], r.wo[0]) + dot(flat[:, half:], r.wo[1])
    r.own[...] = (resid * r.moe_gain[pl.ds(ep, 1), :]).astype(NARROW)
    r.every[ep] = r.own[...]
    for name in ("dg", "du", "eg", "eu"):
        loads[name].wait()
        crossed[name].wait_recv()

    r.squares[...] = jnp.zeros_like(r.squares)
    r.logits[...] = jnp.zeros_like(r.logits)
    ffe = r.eg.shape[2]
    ffd = r.dg.shape[2]

    def absorb(i):
        far = flip(z, i)
        blocks = [r.every[far * square + k] for k in range(square)]
        squares, logits = r.squares[...], r.logits[...]
        for k, v in enumerate(blocks):
            v = v.astype(FULL)
            u = v / r.moe_gain[pl.ds(far * square + k, 1), :]
            squares = squares + u * u
            logits = logits + v * r.mixes[pl.ds(far * square + k, 1), :]
        r.squares[...], r.logits[...] = squares, logits
        left = jnp.concatenate(blocks, axis=1)
        span = pl.ds(pl.multiple_of(far * (square * cols), square * cols), square * cols)
        for dense, expert, low, high in (
            (r.dg, r.eg, r.dgate, r.egate),
            (r.du, r.eu, r.dup, r.eup),
        ):
            pair = jnp.concatenate([dense[0, span, :], dense[1, span, :]], axis=1)
            terms = [(low, 0, pair), (high, 0, expert[0, span, :]), (high, ffe, expert[1, span, :])]
            for ref, start, right in terms:
                lane = slice(start, start + right.shape[1])
                got = dot(left, right)
                if i:
                    got = got + ref[:, lane]
                ref[:, lane] = got

    finish3 = gather(
        count,
        [(r.own, lambda z, b, a: r.every.at[ep_of(side, t, z, b, a)], None)],
        r.ring3,
        absorb,
    )
    scale = jnp.sum(r.squares[...], axis=1, keepdims=True) * (1.0 / width)
    scale = lax.rsqrt(scale + EPS)
    dense_mix = sigmoid(scale * jnp.sum(r.logits[...], axis=1, keepdims=True))
    weight = r.weight[:, :1]
    for gate, up, act, factor in (
        (r.dgate, r.dup, r.dact, dense_mix),
        (r.egate, r.eup, r.eact, weight),
    ):
        step = min(256, act.shape[1])
        for start in range(0, act.shape[1], step):
            lane = slice(start, start + step)
            value = silu(scale * gate[:, lane]) * (scale * up[:, lane] * factor)
            act[:, lane] = value.astype(NARROW)
    for name in ("dd", "ed"):
        loads[name].wait()
        crossed[name].wait_recv()

    chunks, step = r.part.shape[0], r.part.shape[-1]
    started = []

    def send(src, dst, offset):
        device = (ep_of(side, t, *at(here, offset)), t)
        copy = remote(src, dst, r.reduce, len(started), device)
        copy.start()
        started.append(copy)
        return copy

    first, second = {}, {}
    for c in range(chunks):
        span = slice(c * step, (c + 1) * step)
        term = 0.0
        for h in range(2):
            term = term + dot(r.dact[:, h * ffd : (h + 1) * ffd], r.dd[h, :, span])
            term = term + dot(r.eact[:, h * ffe : (h + 1) * ffe], r.ed[h, :, span])
        r.part[c] = term.reshape(r.part.shape[1:]).astype(NARROW)
        for n, offset in enumerate(plane):
            _, b2, a2 = at(here, offset)
            first[c, n] = send(r.part.at[c, :, a2, b2], r.plane_buf.at[c, n], offset)
    line, lane = grid_ids(own_rows, total)
    pick = jnp.where(lane == line + my_slot * own_rows, 1.0, 0.0).astype(NARROW)
    for e in range(count):
        span = slice(e * cols, (e + 1) * cols)
        r.resid[:, span] = dot(pick, r.every[e]) / r.moe_gain[e : e + 1, :]
    for c in range(chunks):
        sums = r.part[c, :, a, b].astype(FULL)
        for n in range(len(plane)):
            first[c, n].wait_recv()
            sums = sums + r.plane_buf[c, n].astype(FULL)
        r.sums[c] = sums.astype(NARROW)
        for n, offset in enumerate(lines):
            second[c, n] = send(r.sums.at[c, flip(z, offset[0])], r.line_buf.at[c, n], offset)
    for c in range(chunks):
        span = slice(c * step, (c + 1) * step)
        sums = r.resid[:, span] + r.sums[c, z].astype(FULL)
        for n in range(len(lines)):
            second[c, n].wait_recv()
            sums = sums + r.line_buf[c, n].astype(FULL)
        for k in range(0, step, 256):
            two = [sums[:, k + j : k + j + 128] for j in (0, 128)]
            first_row = (c * step + k) // 128 * own_rows
            rows = slice(first_row, first_row + 2 * own_rows)
            r.pack[2 * groups + 2, rows] = jnp.concatenate(two, axis=0).astype(NARROW)
    for finish in (finish2, finish3, swap.wait_send):
        finish()
    for copy in list(crossed.values()) + started:
        copy.wait_send()


def update_kernel(groups, pack_ref, state_ref, new_ref, out_ref, keeps):
    bunch, heads, size = state_ref.shape[:3]
    step = pl.program_id(0)
    per = pl.num_programs(0) // groups

    @pl.when(step == 0)
    def _():
        keeps[...] = pack_ref[2 * groups].astype(FULL) + pack_ref[2 * groups + 1].astype(FULL)
        own_rows, width = out_ref.shape
        for e in range(width // 128):
            rows = pack_ref[2 * groups + 2, e * own_rows : (e + 1) * own_rows]
            out_ref[:, e * 128 : (e + 1) * 128] = rows

    tall = pack_ref[step // per]
    across = pack_ref[groups + step // per].astype(FULL)
    row = lax.broadcasted_iota(jnp.int32, across.shape, 0)
    for s in range(bunch):
        place_in = (step % per) * bunch + s
        first = pl.multiple_of((step * bunch + s) * heads, heads)
        keep = keeps[pl.ds(first, heads)]
        for h in range(0, heads, 2):
            wanted = [place_in * (4 * heads) + h + i for i in range(2)]
            two = [
                jnp.where(
                    (row == w) | (row == w + heads) | (row == w + 2 * heads), across, 0.0
                )
                for w in wanted
            ]
            outer = dot(tall, jnp.concatenate(two, axis=1).astype(NARROW))
            for i in range(2):
                kept = keep[h + i : h + i + 1] * state_ref[s, h + i]
                new_ref[s, h + i] = kept + outer[:, i * size : (i + 1) * size]


def update(groups, pack, state, layer):
    seqs, heads, size, _ = state.shape
    bunch = 2
    own = pl.BlockSpec((bunch, heads, size, size), lambda s: (s, 0, 0, 0))
    return pl.pallas_call(
        functools.partial(update_kernel, groups),
        grid=(seqs // bunch,),
        out_shape=(jax.ShapeDtypeStruct(state.shape, state.dtype), layer),
        in_specs=[pl.BlockSpec(pack.shape, lambda s: (0, 0, 0)), own],
        out_specs=(own, pl.BlockSpec(layer.shape, lambda s: (0, 0))),
        scratch_shapes=[VMEM((seqs * heads, size), FULL)],
        compiler_params=pltpu.CompilerParams(
            dimension_semantics=("arbitrary",), vmem_limit_bytes=12 * 1024 * 1024
        ),
        name="update",
    )(pack, state)


def body(
    tokens,
    mix_gain,
    w_query,
    w_key,
    w_value,
    w_zgate,
    w_beta,
    w_decay,
    decay_rate,
    decay_bias,
    head_gain,
    state,
    w_out,
    moe_gain,
    dense_mix,
    dense_gate,
    dense_up,
    dense_down,
    expert_gate,
    expert_up,
    expert_down,
    expert_ids,
    route_weight,
):
    count = lax.axis_size("ep")
    own_rows, width = tokens.shape
    seqs, heads, size, _ = state.shape
    depth, side = grid_of(count)
    total = count * own_rows
    flatten = lambda w: w.transpose(1, 2, 0).reshape(-1, width)
    cols = w_out.shape[1]
    operands = {
        "tokens": tokens,
        "gain": mix_gain.reshape(1, width),
        "beta": w_beta.T,
        "decay": w_decay.T,
        "rate": decay_rate.reshape(1, heads),
        "bias": decay_bias.reshape(1, heads),
        "head_gain": head_gain.reshape(1, size),
        "moe_gain": moe_gain.reshape(count, cols),
        "mix": dense_mix.reshape(count, cols),
        "ids": expert_ids.T,
        "route": route_weight.T,
    }
    split = {
        "wo": w_out,
        "dg": dense_gate,
        "du": dense_up,
        "dd": dense_down,
        "eg": expert_gate[0],
        "eu": expert_up[0],
        "ed": expert_down[0],
    }
    only = {
        "wq": flatten(w_query),
        "wk": flatten(w_key),
        "wv": flatten(w_value),
        "wz": flatten(w_zgate),
        "state": state,
    }
    wide = 4 * only["wq"].shape[0]
    ffd, ffe = dense_gate.shape[1], expert_gate.shape[2]
    chunks = 4
    room = 55 * 1024 if total * width <= 2**18 else 60 * 1024
    step = width // chunks
    group = 128 // (4 * heads)
    near, flat = side * side - 1, depth - 1
    narrow = lambda *shape: VMEM(shape, NARROW)
    full = lambda *shape: VMEM(shape, FULL)
    scratch = {k: VMEM(v.shape, v.dtype) for k, v in operands.items()}
    scratch |= {k: narrow(2, *v.shape) for k, v in split.items()}
    scratch |= {
        "state": full(*state.shape),
        "rows": narrow(count, own_rows, width),
        "pair": narrow(2, own_rows, width),
        "normed": narrow(total, width),
        "weights": narrow(2, wide, width),
        "blocks": narrow(2, count, own_rows, wide),
        "landed": narrow(count, 2, own_rows, wide),
        "flat": full(-(-wide // 128), count * seqs, 128),
        "turned": full(seqs // group, size, 128),
        "columns": full(total, cols),
        "weight": full(total, 128),
        "mixes": full(count, cols),
        "ready": full(6, seqs, heads, size),
        "write": full(seqs, heads, size),
        "acc": full(own_rows * heads, size),
        "gated": narrow(2, own_rows, heads * size),
        "mixed": narrow(count, own_rows, width),
        "own": narrow(total, cols),
        "every": narrow(count, total, cols),
        "squares": full(total, cols),
        "logits": full(total, cols),
        "dgate": full(total, 2 * ffd),
        "dup": full(total, 2 * ffd),
        "egate": full(total, 2 * ffe),
        "eup": full(total, 2 * ffe),
        "dact": narrow(total, 2 * ffd),
        "eact": narrow(total, 2 * ffe),
        "part": narrow(chunks, depth, side, side, own_rows, step),
        "plane_buf": narrow(chunks, max(near, 1), depth, own_rows, step),
        "sums": narrow(chunks, depth, own_rows, step),
        "line_buf": narrow(chunks, max(flat, 1), own_rows, step),
        "resid": full(own_rows, width),
        "load_sem": pltpu.SemaphoreType.DMA((len(operands) + len(split) + 4 + seqs,)),
    }
    pairs = {
        "core": 1 + 4 + len(split) + 1,
        "ring1": count - 1,
        "ring2": 2 * (count - 1),
        "ring3": count - 1,
        "swap": 2 * count - 1,
        "reduce": chunks * (near + flat),
    }
    for name, n in pairs.items():
        scratch[name + "_send"] = pltpu.SemaphoreType.DMA((n,))
        scratch[name + "_recv"] = pltpu.SemaphoreType.DMA((n,))
    sources = operands | split | only
    outs = {"pack": jax.ShapeDtypeStruct((2 * (seqs // group) + 3, 128, 128), NARROW)}
    names = [k + "_hbm" for k in sources] + list(outs) + list(scratch)
    spec = pl.BlockSpec(memory_space=VMEM)
    pack = pl.pallas_call(
        functools.partial(layer_kernel, count, names, tuple(pairs)),
        out_shape=outs["pack"],
        in_specs=[pl.BlockSpec(memory_space=HBM)] * len(sources),
        out_specs=spec,
        scratch_shapes=list(scratch.values()),
        compiler_params=pltpu.CompilerParams(
            collective_id=1, has_side_effects=True, vmem_limit_bytes=room * 1024
        ),
        cost_estimate=pl.CostEstimate(
            flops=4 * 10**10, bytes_accessed=10**8, transcendentals=0
        ),
        name="layer",
    )(*sources.values())
    layer = jax.ShapeDtypeStruct((own_rows, width), NARROW)
    new_state, layer_out = update(seqs // group, pack, state, layer)
    return (layer_out, new_state)


def solution(mesh):
    placed = (
        P(("ep", "tp"), None),
        P(),
        P(None, "tp", "ep"),
        P(None, "tp", "ep"),
        P(None, "tp", "ep"),
        P(None, "tp", "ep"),
        P(None, "tp"),
        P(None, "tp"),
        P("tp"),
        P("tp"),
        P(),
        P("ep", "tp", None, None),
        P("tp", "ep"),
        P(),
        P(),
        P(None, ("ep", "tp")),
        P(None, ("ep", "tp")),
        P(("ep", "tp"), None),
        P("ep", None, "tp"),
        P("ep", None, "tp"),
        P("ep", "tp", None),
        P(),
        P(),
    )
    return jax.shard_map(
        body,
        mesh=mesh,
        in_specs=placed,
        out_specs=(P(("ep", "tp"), None), P("ep", "tp", None, None)),
        check_vma=False,
    )
```

time: 82.3 us -> 68.5 us (0.83)
  Pallas kernels: 79.7 us -> 66.7 us
    pallas_call x3 -> x2, Pallas kernels: 79.7 us -> 66.7 us  [the longest x1 59.9 us: body(): pl.pallas_call(functools.partial(layer_kernel, count, names, tuple(pairs)...]
where the time goes in v2:
time: 68.5 us; the launch traced here: 68.3 us
  Pallas kernels  66.7 us (97%)
  local copies, waits for them, and re-layouts  0.98 us (1%)
    pallas_call x1, Pallas kernels, body(): pl.pallas_call(functools.partial(layer_kernel, count, names, tuple(pairs)...  59.9 us
    pallas_call x1, Pallas kernels, update(): pl.pallas_call(functools.partial(update_kernel, groups), grid=(seqs // bu...  6.76 us

profile of v2, /device:TPU:0, one launch (start us, length us, event | category | flops | bytes accessed | tf_op | source)
XLA Modules:
  0.0 68.3 jit_solution(12416081754660237863)
XLA Ops:
  0.6 0.0 copy-start
  0.7 59.9 %layer.1.pack_ref = bf16[11,128,128]{2,1,0:T(8,128)(2,1)} custom-call(bf16[8,2048]{1,0:T(8,128)(2,1)} %refs_0_.1, f32[1,2048]{1,0:T(1,128)} %bitcast.34, bf16[8,2048]{1,0:T(8,128)(2,1)} %bitcast.32, bf16[8,2048]{1,0:T(8,128)(2,1)} %bitcast.33, f32[1,8]{1,0:T(1,128)} %bitcast.39, f32[1,8]{1,0:T(1,128)} %bitcast.40, f32[1,128]{1,0:T(1,128)} %bitcast.41, ...), custom_call_target="tpu_custom_call" | custom-call | flops 40000000000 | bytes 100000000 | tf_op jit(solution)/shard_map/layer/pallas_call | solution.py:691
  60.6 0.0 copy-done
  60.6 0.0 copy-start.1
  60.6 1.0 %copy-done.1 = bf16[11,128,128]{2,1,0:T(8,128)(2,1)S(1)} copy-done((bf16[11,128,128]{2,1,0:T(8,128)(2,1)S(1)}, bf16[11,128,128]{2,1,0:T(8,128)(2,1)}, u32[]{:S(2)}) %copy-start.1) | copy-done | bytes 360472
  61.6 6.8 %update.1 = (f32[16,8,128,128]{3,2,1,0:T(8,128)}, bf16[8,2048]{1,0:T(8,128)(2,1)}) custom-call(bf16[11,128,128]{2,1,0:T(8,128)(2,1)S(1)} %copy-done.1, f32[16,8,128,128]{3,2,1,0:T(8,128)S(1)} %copy-done), custom_call_target="tpu_custom_call" | custom-call | tf_op jit(solution)/shard_map/update/pallas_call | solution.py:555
Async XLA Ops:
  0.6 59.9 %copy-start = (f32[16,8,128,128]{3,2,1,0:T(8,128)S(1)}, f32[16,8,128,128]{3,2,1,0:T(8,128)}, u32[]{:S(2)}) copy-start(f32[16,8,128,128]{3,2,1,0:T(8,128)} %state_ref.1) | copy-start | bytes 25165828
  60.6 1.0 %copy-start.1 = (bf16[11,128,128]{2,1,0:T(8,128)(2,1)S(1)}, bf16[11,128,128]{2,1,0:T(8,128)(2,1)}, u32[]{:S(2)}) copy-start(bf16[11,128,128]{2,1,0:T(8,128)(2,1)} %layer.1.pack_ref) | copy-start | bytes 1081348

commit v3 on v2

--- a/solution.py
+++ b/solution.py
@@ -94,31 +94,46 @@
     )
 
 
-def gather(count, pieces, sems, landed=None, then=None):
+def gather(count, pieces, sems, whole, landed=None, then=None):
     depth, side, t, *here = place(count)
     lines, plane = peers_of(count)
-    started = []
+    nothing = (0, 0, 0)
+    send_sem, recv_sem = sems
     arrivals = {}
-    nothing = (0, 0, 0)
-    plus = lambda u, v: tuple(i ^ j for i, j in zip(u, v))
+    grouped = len(pieces) * len(lines)
 
     def spread(p, offset, steps):
         source, view, _ = pieces[p]
         spot = view(*at(here, offset))
-        if offset == nothing and source is not None:
-            source_ref = source
-        else:
-            source_ref = spot
         for step in steps:
-            device = (ep_of(side, t, *at(here, step)), t)
-            copy = remote(source_ref, spot, sems, len(started), device)
+            line = step in lines
+            n = p * len(lines) + step[0] - 1 if line else grouped + offset[0]
+            copy = pltpu.make_async_remote_copy(
+                src_ref=source if offset == nothing else spot,
+                dst_ref=spot,
+                send_sem=send_sem.at[0],
+                recv_sem=recv_sem.at[n],
+                device_id=(ep_of(side, t, *at(here, step)), t),
+                device_id_type=MESH,
+            )
             copy.start()
-            started.append(copy)
-            arrivals[p, plus(offset, step)] = copy
-
-    for p, (_, _, arrival) in enumerate(pieces):
-        if arrival is not None:
-            arrival()
+            if line:
+                arrivals[p, step] = copy
+
+    def all_of(blocks, n):
+        span = whole.at[pl.ds(0, blocks)]
+        return pltpu.make_async_remote_copy(
+            src_ref=span,
+            dst_ref=span,
+            send_sem=send_sem.at[0],
+            recv_sem=recv_sem.at[n],
+            device_id=other_core(),
+            device_id_type=MESH,
+        )
+
+    for p, (_, _, first) in enumerate(pieces):
+        if first is not None:
+            first()
         spread(p, nothing, plane + lines)
     if then is not None:
         then()
@@ -127,17 +142,11 @@
             arrivals[p, offset].wait_recv()
             spread(p, offset, plane)
     for offset in [nothing] + lines:
-        for p in range(len(pieces)):
-            for step in plane:
-                arrivals[p, plus(offset, step)].wait_recv()
+        all_of(len(plane), grouped + offset[0]).wait_recv()
         if landed is not None:
             landed(offset[0])
 
-    def finish():
-        for copy in started:
-            copy.wait_send()
-
-    return finish
+    return lambda: all_of(count - 1, 0).wait_send()
 
 
 def contract(left, right):
@@ -198,11 +207,11 @@
     spot_of = lambda p: r.weights.at[t, pl.ds(p * per, per)]
     for p, src in enumerate(projections):
         load(("w", p), src, spot_of(p))
-    for s in range(seqs):
-        load(("state", s), r.state_hbm.at[s], r.state.at[s])
+    load("state", r.state_hbm, r.state)
     for name in late:
         load(name, getattr(r, name + "_hbm"), getattr(r, name))
-    shards = ("wo", "dg", "du", "eg", "eu", "dd", "ed")
+    early, later = ("wo", "dg", "du", "eg"), ("eu", "dd", "ed")
+    shards = early + later
     for name in shards:
         load(name, getattr(r, name + "_hbm"), getattr(r, name).at[t])
 
@@ -210,10 +219,6 @@
     devices = [partner] + [(ep_of(side, t, *at(here, o)), t) for o in plane + lines]
     for device in devices:
         pl.semaphore_signal(barrier, inc=1, device_id=device, device_id_type=MESH)
-    source, target = grid_ids(wide, wide)
-    inner = source % per
-    spot = inner % part * (4 * heads) + source // per * heads + inner // part
-    order = jnp.where(target == spot, 1.0, 0.0).astype(NARROW)
     loads["tokens"].wait()
     r.rows[my_slot] = r.tokens[...]
     r.pair[t] = r.tokens[...]
@@ -226,10 +231,19 @@
         copy.start()
         crossed[name] = copy
 
+    def order_ready():
+        source, target = grid_ids(wide, wide)
+        inner = source % per
+        spot = inner % part * (4 * heads) + source // per * heads + inner // part
+        r.order[...] = jnp.where(target == spot, 1.0, 0.0).astype(NARROW)
+
     def begin():
         cross("pair", r.tokens, r.pair.at[t])
         for p, src in enumerate(projections):
             cross(("w", p), src, spot_of(p))
+        for name in early:
+            cross(name, getattr(r, name + "_hbm"), getattr(r, name).at[t])
+        order_ready()
 
     loads["gain"].wait()
     gain = r.gain[...]
@@ -243,22 +257,27 @@
             two = rms_scale(jnp.concatenate(two, axis=0), gain).astype(NARROW)
             start = pl.multiple_of(first * own_rows, 2 * own_rows)
             r.normed[pl.ds(start, 2 * own_rows)] = two
+        if i == 0:
+            for p in range(4):
+                loads["w", p].wait()
+                crossed["w", p].wait_recv()
+            order = r.order[...]
+            for h in range(2):
+                r.ordered[h] = lax.dot_general(
+                    r.weights[h],
+                    order,
+                    (((0,), (0,)), ((), ())),
+                    preferred_element_type=FULL,
+                ).astype(NARROW)
 
     finish1 = gather(
-        count, [(r.tokens, slots(r.rows), None)], r.ring1, normalise, then=begin
+        count, [(r.tokens, slots(r.rows), None)], r.ring1, r.rows, normalise, then=begin
     )
-    for p in range(4):
-        loads["w", p].wait()
-        crossed["w", p].wait_recv()
-    for name in shards:
-        cross(name, getattr(r, name + "_hbm"), getattr(r, name).at[t])
     left = r.normed[...]
     for h in range(2):
-        product = contract(left, r.weights[h]).astype(NARROW)
-        moved = dot(product, order)
-        r.blocks[h] = moved.reshape(count, own_rows, wide).astype(NARROW)
-
-    exchange = []
+        product = dot(left, r.ordered[h])
+        r.blocks[h] = product.reshape(count, own_rows, wide).astype(NARROW)
+
     for offset in [(i, j, k) for i in range(depth) for j in range(side) for k in range(side)][::-1]:
         z2, b2, a2 = at(here, offset)
         other = ep_of(side, t, z2, b2, a2)
@@ -266,12 +285,12 @@
         for core in (1 - t, t):
             if offset == (0, 0, 0) and core is t:
                 continue
-            copy = remote(
-                r.blocks.at[core, row], r.landed.at[ep, t], r.swap, len(exchange), (other, core)
-            )
-            copy.start()
-            exchange.append(copy)
-    r.landed[ep, t] = r.blocks[t, my_slot]
+            remote(
+                r.blocks.at[core, row], r.landed.at[2 * ep + t], r.swap, 0, (other, core)
+            ).start()
+    r.landed[2 * ep + t] = r.blocks[t, my_slot]
+    most = r.landed.at[pl.ds(0, 2 * count - 1)]
+    exchange = remote(most, most, r.swap, 0, partner)
 
     if cols % 128 == 0:
         span = pl.ds(pl.multiple_of(ep * cols, 128), cols)
@@ -304,10 +323,8 @@
     r.weight[...] = jnp.broadcast_to(weight, r.weight.shape)
     r.mixes[...] = r.mix[...].astype(FULL)
     finish1()
-    for s in range(seqs):
-        loads["state", s].wait()
-    for copy in exchange:
-        copy.wait()
+    loads["state"].wait()
+    exchange.wait()
 
     lanes = 4 * heads
     bunch = 128 // lanes
@@ -337,7 +354,6 @@
 
     there = slot_of(depth, side, *place_of(count, ep, 1 - t))
     mine = pl.ds(pl.multiple_of(t * half, half), half)
-    others = pl.ds(pl.multiple_of((1 - t) * half, half), half)
     head_gain = r.head_gain[...]
     line = lax.broadcasted_iota(jnp.int32, (2 * heads, size), 0) % heads
 
@@ -370,19 +386,25 @@
             r.gated[core, :, h * size : (h + 1) * size] = piece.astype(NARROW)
 
     readouts(1 - t)
-    swap = remote(r.gated.at[1 - t], r.mixed.at[there, :, mine], r.core, len(crossed), partner)
+    swap = remote(
+        r.gated.at[1 - t], r.mixed.at[there, :, mine], r.core, 5 + len(shards), partner
+    )
     swap.start()
+    for name in later:
+        cross(name, getattr(r, name + "_hbm"), getattr(r, name).at[t])
     readouts(t)
     r.mixed[my_slot, :, mine] = r.gated[t]
 
-    view = lambda span: lambda z, b, a: r.mixed.at[slot_of(depth, side, z, b, a), :, span]
-
     groups = seqs // bunch
+    stores = [
+        pltpu.make_async_copy(r.packed.at[span], r.pack.at[span], r.store_sem.at[i])
+        for i, span in enumerate((pl.ds(0, 2 * groups + 2), pl.ds(2 * groups + 2, 1)))
+    ]
 
     def prepare():
         keep = r.ready[5].reshape(seqs * heads, size)
-        r.pack[2 * groups] = keep.astype(NARROW)
-        r.pack[2 * groups + 1] = (keep - keep.astype(NARROW).astype(FULL)).astype(NARROW)
+        r.packed[2 * groups] = keep.astype(NARROW)
+        r.packed[2 * groups + 1] = (keep - keep.astype(NARROW).astype(FULL)).astype(NARROW)
         none = jnp.zeros((heads, size), FULL)
         high = lambda v: v.astype(NARROW).astype(FULL)
         for g in range(groups):
@@ -391,13 +413,18 @@
                 key, write = r.ready[1, s], r.write[s]
                 tall += [high(key), high(key), key - high(key), none]
                 across += [high(write), write - high(write), high(write), none]
-            r.pack[g] = jnp.transpose(jnp.concatenate(tall, axis=0)).astype(NARROW)
-            r.pack[groups + g] = jnp.concatenate(across, axis=0).astype(NARROW)
-
+            r.packed[g] = jnp.transpose(jnp.concatenate(tall, axis=0)).astype(NARROW)
+            r.packed[groups + g] = jnp.concatenate(across, axis=0).astype(NARROW)
+        stores[0].start()
+
+    others = pl.ds(pl.multiple_of((1 - t) * half, half), half)
+    part_of = lambda span: lambda z, b, a: r.mixed.at[slot_of(depth, side, z, b, a), :, span]
+    came = r.mixed.at[my_slot, :, others]
     finish2 = gather(
         count,
-        [(r.gated.at[t], view(mine), None), (None, view(others), swap.wait_recv)],
+        [(r.gated.at[t], part_of(mine), None), (came, part_of(others), swap.wait_recv)],
         r.ring2,
+        r.mixed,
         then=prepare,
     )
     loads["wo"].wait()
@@ -444,6 +471,7 @@
         count,
         [(r.own, lambda z, b, a: r.every.at[ep_of(side, t, z, b, a)], None)],
         r.ring3,
+        r.every,
         absorb,
     )
     scale = jnp.sum(r.squares[...], axis=1, keepdims=True) * (1.0 / width)
@@ -464,26 +492,46 @@
         crossed[name].wait_recv()
 
     chunks, step = r.part.shape[0], r.part.shape[-1]
-    started = []
-
-    def send(src, dst, offset):
-        device = (ep_of(side, t, *at(here, offset)), t)
-        copy = remote(src, dst, r.reduce, len(started), device)
-        copy.start()
-        started.append(copy)
-        return copy
-
-    first, second = {}, {}
+
+    def send(src, dst, offset, kind, c):
+        pltpu.make_async_remote_copy(
+            src_ref=src,
+            dst_ref=dst,
+            send_sem=r.reduce[0].at[kind],
+            recv_sem=r.reduce[1].at[kind * chunks + c],
+            device_id=(ep_of(side, t, *at(here, offset)), t),
+            device_id_type=MESH,
+        ).start()
+
+    def arrived_all(ref, kind, c):
+        pltpu.make_async_remote_copy(
+            src_ref=ref,
+            dst_ref=ref,
+            send_sem=r.reduce[0].at[kind],
+            recv_sem=r.reduce[1].at[kind * chunks + c],
+            device_id=partner,
+            device_id_type=MESH,
+        ).wait_recv()
+
+    def sent_all(ref, kind):
+        pltpu.make_async_remote_copy(
+            src_ref=ref,
+            dst_ref=ref,
+            send_sem=r.reduce[0].at[kind],
+            recv_sem=r.reduce[1].at[0],
+            device_id=partner,
+            device_id_type=MESH,
+        ).wait_send()
+
     for c in range(chunks):
         span = slice(c * step, (c + 1) * step)
-        term = 0.0
-        for h in range(2):
-            term = term + dot(r.dact[:, h * ffd : (h + 1) * ffd], r.dd[h, :, span])
-            term = term + dot(r.eact[:, h * ffe : (h + 1) * ffe], r.ed[h, :, span])
+        dense = r.dd[:, :, span].reshape(2 * ffd, step)
+        expert = r.ed[:, :, span].reshape(2 * ffe, step)
+        term = dot(r.dact[...], dense) + dot(r.eact[...], expert)
         r.part[c] = term.reshape(r.part.shape[1:]).astype(NARROW)
         for n, offset in enumerate(plane):
             _, b2, a2 = at(here, offset)
-            first[c, n] = send(r.part.at[c, :, a2, b2], r.plane_buf.at[c, n], offset)
+            send(r.part.at[c, :, a2, b2], r.plane_buf.at[c, n], offset, 0, c)
     line, lane = grid_ids(own_rows, total)
     pick = jnp.where(lane == line + my_slot * own_rows, 1.0, 0.0).astype(NARROW)
     for e in range(count):
@@ -491,33 +539,37 @@
         r.resid[:, span] = dot(pick, r.every[e]) / r.moe_gain[e : e + 1, :]
     for c in range(chunks):
         sums = r.part[c, :, a, b].astype(FULL)
+        arrived_all(r.plane_buf.at[c], 0, c)
         for n in range(len(plane)):
-            first[c, n].wait_recv()
             sums = sums + r.plane_buf[c, n].astype(FULL)
         r.sums[c] = sums.astype(NARROW)
         for n, offset in enumerate(lines):
-            second[c, n] = send(r.sums.at[c, flip(z, offset[0])], r.line_buf.at[c, n], offset)
+            send(r.sums.at[c, flip(z, offset[0])], r.line_buf.at[c, n], offset, 1, c)
     for c in range(chunks):
         span = slice(c * step, (c + 1) * step)
         sums = r.resid[:, span] + r.sums[c, z].astype(FULL)
+        arrived_all(r.line_buf.at[c], 1, c)
         for n in range(len(lines)):
-            second[c, n].wait_recv()
             sums = sums + r.line_buf[c, n].astype(FULL)
         for k in range(0, step, 256):
             two = [sums[:, k + j : k + j + 128] for j in (0, 128)]
             first_row = (c * step + k) // 128 * own_rows
             rows = slice(first_row, first_row + 2 * own_rows)
-            r.pack[2 * groups + 2, rows] = jnp.concatenate(two, axis=0).astype(NARROW)
+            r.packed[2 * groups + 2, rows] = jnp.concatenate(two, axis=0).astype(NARROW)
+    stores[1].start()
+    stores[0].wait()
     for finish in (finish2, finish3, swap.wait_send):
         finish()
-    for copy in list(crossed.values()) + started:
+    for copy in crossed.values():
         copy.wait_send()
+    sent_all(r.plane_buf, 0)
+    sent_all(r.line_buf, 1)
+    stores[1].wait()
 
 
 def update_kernel(groups, pack_ref, state_ref, new_ref, out_ref, keeps):
     bunch, heads, size = state_ref.shape[:3]
     step = pl.program_id(0)
-    per = pl.num_programs(0) // groups
 
     @pl.when(step == 0)
     def _():
@@ -527,22 +579,18 @@
             rows = pack_ref[2 * groups + 2, e * own_rows : (e + 1) * own_rows]
             out_ref[:, e * 128 : (e + 1) * 128] = rows
 
-    tall = pack_ref[step // per]
-    across = pack_ref[groups + step // per].astype(FULL)
-    row = lax.broadcasted_iota(jnp.int32, across.shape, 0)
+    tall = pack_ref[step]
+    across = pack_ref[groups + step].astype(FULL)
+    rank = 4 * heads
+    row = lax.broadcasted_iota(jnp.int32, (rank, size), 0) % heads
     for s in range(bunch):
-        place_in = (step % per) * bunch + s
+        left = tall[:, s * rank : (s + 1) * rank]
+        right = across[s * rank : (s + 1) * rank]
         first = pl.multiple_of((step * bunch + s) * heads, heads)
         keep = keeps[pl.ds(first, heads)]
         for h in range(0, heads, 2):
-            wanted = [place_in * (4 * heads) + h + i for i in range(2)]
-            two = [
-                jnp.where(
-                    (row == w) | (row == w + heads) | (row == w + 2 * heads), across, 0.0
-                )
-                for w in wanted
-            ]
-            outer = dot(tall, jnp.concatenate(two, axis=1).astype(NARROW))
+            two = [jnp.where(row == h + i, right, 0.0) for i in range(2)]
+            outer = dot(left, jnp.concatenate(two, axis=1).astype(NARROW))
             for i in range(2):
                 kept = keep[h + i : h + i + 1] * state_ref[s, h + i]
                 new_ref[s, h + i] = kept + outer[:, i * size : (i + 1) * size]
@@ -550,7 +598,7 @@
 
 def update(groups, pack, state, layer):
     seqs, heads, size, _ = state.shape
-    bunch = 2
+    bunch = seqs // groups
     own = pl.BlockSpec((bunch, heads, size, size), lambda s: (s, 0, 0, 0))
     return pl.pallas_call(
         functools.partial(update_kernel, groups),
@@ -560,7 +608,7 @@
         out_specs=(own, pl.BlockSpec(layer.shape, lambda s: (0, 0))),
         scratch_shapes=[VMEM((seqs * heads, size), FULL)],
         compiler_params=pltpu.CompilerParams(
-            dimension_semantics=("arbitrary",), vmem_limit_bytes=12 * 1024 * 1024
+            dimension_semantics=("arbitrary",), vmem_limit_bytes=16 * 1024 * 1024
         ),
         name="update",
     )(pack, state)
@@ -644,8 +692,10 @@
         "pair": narrow(2, own_rows, width),
         "normed": narrow(total, width),
         "weights": narrow(2, wide, width),
+        "order": narrow(wide, wide),
+        "ordered": narrow(2, width, wide),
         "blocks": narrow(2, count, own_rows, wide),
-        "landed": narrow(count, 2, own_rows, wide),
+        "landed": narrow(2 * count, own_rows, wide),
         "flat": full(-(-wide // 128), count * seqs, 128),
         "turned": full(seqs // group, size, 128),
         "columns": full(total, cols),
@@ -671,27 +721,29 @@
         "sums": narrow(chunks, depth, own_rows, step),
         "line_buf": narrow(chunks, max(flat, 1), own_rows, step),
         "resid": full(own_rows, width),
-        "load_sem": pltpu.SemaphoreType.DMA((len(operands) + len(split) + 4 + seqs,)),
+        "packed": narrow(2 * (seqs // group) + 3, 128, 128),
+        "store_sem": pltpu.SemaphoreType.DMA((2,)),
+        "load_sem": pltpu.SemaphoreType.DMA((len(operands) + len(split) + 5,)),
     }
     pairs = {
-        "core": 1 + 4 + len(split) + 1,
-        "ring1": count - 1,
-        "ring2": 2 * (count - 1),
-        "ring3": count - 1,
-        "swap": 2 * count - 1,
-        "reduce": chunks * (near + flat),
+        "core": (6 + len(split), 6 + len(split)),
+        "ring1": (1, 2 * depth - 1),
+        "ring2": (1, 3 * depth - 2),
+        "ring3": (1, 2 * depth - 1),
+        "swap": (1, 1),
+        "reduce": (2, 2 * chunks),
     }
-    for name, n in pairs.items():
+    for name, (n, m) in pairs.items():
         scratch[name + "_send"] = pltpu.SemaphoreType.DMA((n,))
-        scratch[name + "_recv"] = pltpu.SemaphoreType.DMA((n,))
+        scratch[name + "_recv"] = pltpu.SemaphoreType.DMA((m,))
     sources = operands | split | only
     outs = {"pack": jax.ShapeDtypeStruct((2 * (seqs // group) + 3, 128, 128), NARROW)}
     names = [k + "_hbm" for k in sources] + list(outs) + list(scratch)
-    spec = pl.BlockSpec(memory_space=VMEM)
+    spec = pl.BlockSpec(memory_space=HBM)
     pack = pl.pallas_call(
         functools.partial(layer_kernel, count, names, tuple(pairs)),
         out_shape=outs["pack"],
-        in_specs=[pl.BlockSpec(memory_space=HBM)] * len(sources),
+        in_specs=[spec] * len(sources),
         out_specs=spec,
         scratch_shapes=list(scratch.values()),
         compiler_params=pltpu.CompilerParams(

time: 68.5 us -> 56.7 us (0.83)
  Pallas kernels: 66.7 us -> 54.9 us
    pallas_call x1, Pallas kernels: 59.9 us -> 50.7 us  [body(): pl.pallas_call(functools.partial(layer_kernel, count, names, tuple(pairs)...]
    pallas_call x1, Pallas kernels: 6.76 us -> 4.17 us  [update(): pl.pallas_call(functools.partial(update_kernel, groups), grid=(seqs // bu...]
where the time goes in v3:
time: 56.7 us; the launch traced here: 56.5 us
  Pallas kernels  54.9 us (97%)
  local copies, waits for them, and re-layouts  0.98 us (2%)
  between operations  0.67 us (1%)
    pallas_call x1, Pallas kernels, body(): pl.pallas_call(functools.partial(layer_kernel, count, names, tuple(pairs)...  50.7 us
    pallas_call x1, Pallas kernels, update(): pl.pallas_call(functools.partial(update_kernel, groups), grid=(seqs // bu...  4.17 us

profile of v3, /device:TPU:0, one launch (start us, length us, event | category | flops | bytes accessed | tf_op | source)
XLA Modules:
  0.0 56.5 jit_solution(9119973646103611081)
XLA Ops:
  0.6 0.0 copy-start
  0.7 50.7 %layer.1.pack_ref = bf16[11,128,128]{2,1,0:T(8,128)(2,1)} custom-call(bf16[8,2048]{1,0:T(8,128)(2,1)} %refs_0_.1, f32[1,2048]{1,0:T(1,128)} %bitcast.34, bf16[8,2048]{1,0:T(8,128)(2,1)} %bitcast.32, bf16[8,2048]{1,0:T(8,128)(2,1)} %bitcast.33, f32[1,8]{1,0:T(1,128)} %bitcast.39, f32[1,8]{1,0:T(1,128)} %bitcast.40, f32[1,128]{1,0:T(1,128)} %bitcast.41, ...), custom_call_target="tpu_custom_call" | custom-call | flops 40000000000 | bytes 100000000 | tf_op jit(solution)/shard_map/layer/pallas_call | solution.py:743
  51.4 0.0 copy-done
  51.4 0.0 copy-start.1
  51.4 1.0 %copy-done.1 = bf16[11,128,128]{2,1,0:T(8,128)(2,1)S(1)} copy-done((bf16[11,128,128]{2,1,0:T(8,128)(2,1)S(1)}, bf16[11,128,128]{2,1,0:T(8,128)(2,1)}, u32[]{:S(2)}) %copy-start.1) | copy-done | bytes 360472
  52.4 4.2 %update.1 = (f32[16,8,128,128]{3,2,1,0:T(8,128)}, bf16[8,2048]{1,0:T(8,128)(2,1)}) custom-call(bf16[11,128,128]{2,1,0:T(8,128)(2,1)S(1)} %copy-done.1, f32[16,8,128,128]{3,2,1,0:T(8,128)S(1)} %copy-done), custom_call_target="tpu_custom_call" | custom-call | tf_op jit(solution)/shard_map/update/pallas_call | solution.py:603
Async XLA Ops:
  0.6 50.7 %copy-start = (f32[16,8,128,128]{3,2,1,0:T(8,128)S(1)}, f32[16,8,128,128]{3,2,1,0:T(8,128)}, u32[]{:S(2)}) copy-start(f32[16,8,128,128]{3,2,1,0:T(8,128)} %state_ref.1) | copy-start | bytes 25165828
  51.4 1.0 %copy-start.1 = (bf16[11,128,128]{2,1,0:T(8,128)(2,1)S(1)}, bf16[11,128,128]{2,1,0:T(8,128)(2,1)}, u32[]{:S(2)}) copy-start(bf16[11,128,128]{2,1,0:T(8,128)(2,1)} %layer.1.pack_ref) | copy-start | bytes 1081348

commit v4 on v3

--- a/solution.py
+++ b/solution.py
@@ -13,6 +13,7 @@
 HBM = pltpu.HBM
 MESH = pl.DeviceIdType.MESH
 NARROW, FULL = jnp.bfloat16, jnp.float32
+TURNED = (3,)
 
 
 def rms_scale(values, gain):
@@ -81,6 +82,10 @@
 
 def at(here, offset):
     return tuple(flip(v, i) for v, i in zip(here, offset))
+
+
+def plus(u, v):
+    return tuple(i ^ j for i, j in zip(u, v))
 
 
 def remote(src, dst, sems, n, device):
@@ -97,31 +102,35 @@
 def gather(count, pieces, sems, whole, landed=None, then=None):
     depth, side, t, *here = place(count)
     lines, plane = peers_of(count)
+    straight = [o for o in plane if not (o[1] and o[2])]
+    corner = [o for o in plane if o[1] and o[2]]
+    turned = [o for o in lines if o[0] in TURNED]
     nothing = (0, 0, 0)
     send_sem, recv_sem = sems
-    arrivals = {}
     grouped = len(pieces) * len(lines)
+    alone = grouped + depth
 
     def spread(p, offset, steps):
         source, view, _ = pieces[p]
         spot = view(*at(here, offset))
         for step in steps:
-            line = step in lines
-            n = p * len(lines) + step[0] - 1 if line else grouped + offset[0]
-            copy = pltpu.make_async_remote_copy(
+            to = plus(offset, step)
+            if to in lines:
+                n = p * len(lines) + to[0] - 1
+            elif to in corner:
+                n = alone + p * len(corner) + corner.index(to)
+            else:
+                n = grouped + to[0]
+            pltpu.make_async_remote_copy(
                 src_ref=source if offset == nothing else spot,
                 dst_ref=spot,
                 send_sem=send_sem.at[0],
                 recv_sem=recv_sem.at[n],
                 device_id=(ep_of(side, t, *at(here, step)), t),
                 device_id_type=MESH,
-            )
-            copy.start()
-            if line:
-                arrivals[p, step] = copy
-
-    def all_of(blocks, n):
-        span = whole.at[pl.ds(0, blocks)]
+            ).start()
+
+    def wait(span, n):
         return pltpu.make_async_remote_copy(
             src_ref=span,
             dst_ref=span,
@@ -131,22 +140,32 @@
             device_id_type=MESH,
         )
 
+    def pass_on(p, offset, n, steps):
+        wait(pieces[p][1](*at(here, offset)), n).wait_recv()
+        spread(p, offset, steps)
+
     for p, (_, _, first) in enumerate(pieces):
         if first is not None:
             first()
         spread(p, nothing, plane + lines)
     if then is not None:
         then()
-    for offset in lines:
+    for i, offset in enumerate(lines):
         for p in range(len(pieces)):
-            arrivals[p, offset].wait_recv()
-            spread(p, offset, plane)
+            steps = straight if offset in turned else plane
+            pass_on(p, offset, p * len(lines) + offset[0] - 1, steps)
+        if i == 0:
+            for p in range(len(pieces)):
+                for k, far in enumerate(corner):
+                    pass_on(p, far, alone + p * len(corner) + k, turned)
     for offset in [nothing] + lines:
-        all_of(len(plane), grouped + offset[0]).wait_recv()
+        blocks = len(straight) if offset == nothing else len(plane)
+        wait(whole.at[pl.ds(0, blocks)], grouped + offset[0]).wait_recv()
         if landed is not None:
             landed(offset[0])
 
-    return lambda: all_of(count - 1, 0).wait_send()
+    whole_send = wait(whole.at[pl.ds(0, count - 1)], 0)
+    return whole_send.wait_send
 
 
 def contract(left, right):
@@ -682,6 +701,7 @@
     step = width // chunks
     group = 128 // (4 * heads)
     near, flat = side * side - 1, depth - 1
+    corners = (side - 1) ** 2
     narrow = lambda *shape: VMEM(shape, NARROW)
     full = lambda *shape: VMEM(shape, FULL)
     scratch = {k: VMEM(v.shape, v.dtype) for k, v in operands.items()}
@@ -727,9 +747,9 @@
     }
     pairs = {
         "core": (6 + len(split), 6 + len(split)),
-        "ring1": (1, 2 * depth - 1),
-        "ring2": (1, 3 * depth - 2),
-        "ring3": (1, 2 * depth - 1),
+        "ring1": (1, 2 * depth - 1 + corners),
+        "ring2": (1, 3 * depth - 2 + 2 * corners),
+        "ring3": (1, 2 * depth - 1 + corners),
         "swap": (1, 1),
         "reduce": (2, 2 * chunks),
     }

time: 56.7 us -> 54.5 us (0.961)
  Pallas kernels: 54.9 us -> 52.7 us
    pallas_call x1, Pallas kernels: 50.7 us -> 48.5 us  [body(): pl.pallas_call(functools.partial(layer_kernel, count, names, tuple(pairs)...]
where the time goes in v4:
time: 54.5 us; the launch traced here: 54.3 us
  Pallas kernels  52.7 us (97%)
  local copies, waits for them, and re-layouts  0.98 us (2%)
  between operations  0.67 us (1%)
    pallas_call x1, Pallas kernels, body(): pl.pallas_call(functools.partial(layer_kernel, count, names, tuple(pairs)...  48.5 us
    pallas_call x1, Pallas kernels, update(): pl.pallas_call(functools.partial(update_kernel, groups), grid=(seqs // bu...  4.17 us

profile of v4, /device:TPU:0, one launch (start us, length us, event | category | flops | bytes accessed | tf_op | source)
XLA Modules:
  0.0 54.3 jit_solution(1639330389149571637)
XLA Ops:
  0.6 0.0 copy-start
  0.7 48.5 %layer.1.pack_ref = bf16[11,128,128]{2,1,0:T(8,128)(2,1)} custom-call(bf16[8,2048]{1,0:T(8,128)(2,1)} %refs_0_.1, f32[1,2048]{1,0:T(1,128)} %bitcast.34, bf16[8,2048]{1,0:T(8,128)(2,1)} %bitcast.32, bf16[8,2048]{1,0:T(8,128)(2,1)} %bitcast.33, f32[1,8]{1,0:T(1,128)} %bitcast.39, f32[1,8]{1,0:T(1,128)} %bitcast.40, f32[1,128]{1,0:T(1,128)} %bitcast.41, ...), custom_call_target="tpu_custom_call" | custom-call | flops 40000000000 | bytes 100000000 | tf_op jit(solution)/shard_map/layer/pallas_call | solution.py:763
  49.2 0.0 copy-done
  49.2 0.0 copy-start.1
  49.2 1.0 %copy-done.1 = bf16[11,128,128]{2,1,0:T(8,128)(2,1)S(1)} copy-done((bf16[11,128,128]{2,1,0:T(8,128)(2,1)S(1)}, bf16[11,128,128]{2,1,0:T(8,128)(2,1)}, u32[]{:S(2)}) %copy-start.1) | copy-done | bytes 360472
  50.2 4.2 %update.1 = (f32[16,8,128,128]{3,2,1,0:T(8,128)}, bf16[8,2048]{1,0:T(8,128)(2,1)}) custom-call(bf16[11,128,128]{2,1,0:T(8,128)(2,1)S(1)} %copy-done.1, f32[16,8,128,128]{3,2,1,0:T(8,128)S(1)} %copy-done), custom_call_target="tpu_custom_call" | custom-call | tf_op jit(solution)/shard_map/update/pallas_call | solution.py:622
Async XLA Ops:
  0.6 48.5 %copy-start = (f32[16,8,128,128]{3,2,1,0:T(8,128)S(1)}, f32[16,8,128,128]{3,2,1,0:T(8,128)}, u32[]{:S(2)}) copy-start(f32[16,8,128,128]{3,2,1,0:T(8,128)} %state_ref.1) | copy-start | bytes 25165828
  49.2 1.0 %copy-start.1 = (bf16[11,128,128]{2,1,0:T(8,128)(2,1)S(1)}, bf16[11,128,128]{2,1,0:T(8,128)(2,1)}, u32[]{:S(2)}) copy-start(bf16[11,128,128]{2,1,0:T(8,128)(2,1)} %layer.1.pack_ref) | copy-start | bytes 1081348

commit v5 on v4

--- a/solution.py
+++ b/solution.py
@@ -562,7 +562,7 @@
         for n in range(len(plane)):
             sums = sums + r.plane_buf[c, n].astype(FULL)
         r.sums[c] = sums.astype(NARROW)
-        for n, offset in enumerate(lines):
+        for n, offset in reversed(list(enumerate(lines))):
             send(r.sums.at[c, flip(z, offset[0])], r.line_buf.at[c, n], offset, 1, c)
     for c in range(chunks):
         span = slice(c * step, (c + 1) * step)

time: 54.5 us -> 54.3 us (level)
  no operation moved by 1% of the time
where the time goes in v5:
time: 54.3 us; the launch traced here: 54.2 us
  Pallas kernels  52.5 us (97%)
  local copies, waits for them, and re-layouts  0.98 us (2%)
  between operations  0.67 us (1%)
    pallas_call x1, Pallas kernels, body(): pl.pallas_call(functools.partial(layer_kernel, count, names, tuple(pairs)...  48.3 us
    pallas_call x1, Pallas kernels, update(): pl.pallas_call(functools.partial(update_kernel, groups), grid=(seqs // bu...  4.17 us

profile of v5, /device:TPU:0, one launch (start us, length us, event | category | flops | bytes accessed | tf_op | source)
XLA Modules:
  0.0 54.2 jit_solution(14148511322873095094)
XLA Ops:
  0.6 0.0 copy-start
  0.7 48.3 %layer.1.pack_ref = bf16[11,128,128]{2,1,0:T(8,128)(2,1)} custom-call(bf16[8,2048]{1,0:T(8,128)(2,1)} %refs_0_.1, f32[1,2048]{1,0:T(1,128)} %bitcast.34, bf16[8,2048]{1,0:T(8,128)(2,1)} %bitcast.32, bf16[8,2048]{1,0:T(8,128)(2,1)} %bitcast.33, f32[1,8]{1,0:T(1,128)} %bitcast.39, f32[1,8]{1,0:T(1,128)} %bitcast.40, f32[1,128]{1,0:T(1,128)} %bitcast.41, ...), custom_call_target="tpu_custom_call" | custom-call | flops 40000000000 | bytes 100000000 | tf_op jit(solution)/shard_map/layer/pallas_call | solution.py:763
  49.0 0.0 copy-done
  49.0 0.0 copy-start.1
  49.0 1.0 %copy-done.1 = bf16[11,128,128]{2,1,0:T(8,128)(2,1)S(1)} copy-done((bf16[11,128,128]{2,1,0:T(8,128)(2,1)S(1)}, bf16[11,128,128]{2,1,0:T(8,128)(2,1)}, u32[]{:S(2)}) %copy-start.1) | copy-done | bytes 360472
  50.0 4.2 %update.1 = (f32[16,8,128,128]{3,2,1,0:T(8,128)}, bf16[8,2048]{1,0:T(8,128)(2,1)}) custom-call(bf16[11,128,128]{2,1,0:T(8,128)(2,1)S(1)} %copy-done.1, f32[16,8,128,128]{3,2,1,0:T(8,128)S(1)} %copy-done), custom_call_target="tpu_custom_call" | custom-call | tf_op jit(solution)/shard_map/update/pallas_call | solution.py:622
Async XLA Ops:
  0.6 48.4 %copy-start = (f32[16,8,128,128]{3,2,1,0:T(8,128)S(1)}, f32[16,8,128,128]{3,2,1,0:T(8,128)}, u32[]{:S(2)}) copy-start(f32[16,8,128,128]{3,2,1,0:T(8,128)} %state_ref.1) | copy-start | bytes 25165828
  49.0 1.0 %copy-start.1 = (bf16[11,128,128]{2,1,0:T(8,128)(2,1)S(1)}, bf16[11,128,128]{2,1,0:T(8,128)(2,1)}, u32[]{:S(2)}) copy-start(bf16[11,128,128]{2,1,0:T(8,128)(2,1)} %layer.1.pack_ref) | copy-start | bytes 1081348
